TPU v7x, 128 devices: a whole 4x4x4 slice. The times are simulated.
128 devices in a mesh: ep: 32 (over z, y, core), tp: 4 (over x).
Axes of the slice: x: 4, y: 4, z: 4, core: 2. Of those that a mesh axis runs over, the one named last changes fastest.
Arguments:
- pool_in: bfloat16 [32768, 1024], P(('ep', 'tp')), may hold values from -6 to 6
- pool_map: bfloat16 [4, 256, 256], replicated, may hold values from -0.375 to 0.375
- pool_scale: float32 [1024], replicated, may hold values from 0.1 to 1.9
- w_out: bfloat16 [1024, 2048], replicated, may hold values from -0.1875 to 0.1875
- mix_gain: float32 [2048], replicated, may hold values from 0.1 to 1.9
- ffn_in: bfloat16 [16384, 2048], P(('ep', 'tp')), may hold values from -6 to 6
- ffn_gain: float32 [2048], replicated, may hold values from 0.1 to 1.9
- routes: int32 [16384, 2], P(('ep', 'tp')), may hold values from 0 to 31, all different within a row; in each aligned block of 128 rows (0 to 127, 128 to 255, ...) at most 10 rows name the same one
- route_weight: float32 [16384, 2], P(('ep', 'tp')), may hold values from 0.1 to 1
- w_gate: bfloat16 [32, 2048, 5632], P('ep', None, 'tp'), may hold values from -0.125 to 0.125
- w_up: bfloat16 [32, 2048, 5632], P('ep', None, 'tp'), may hold values from -0.125 to 0.125
- w_down: bfloat16 [32, 5632, 2048], P('ep', 'tp'), may hold values from -0.078125 to 0.078125
- out_gain: float32 [2048], replicated, may hold values from 0.1 to 1.9
Outputs:
- mixer_out: bfloat16 [32768, 2048], P(('ep', 'tp'))
- moe_out: bfloat16 [16384, 2048], P(('ep', 'tp'))
Inputs may be any that keep to these rules, and one draw needn't show every extreme that they name: `routes`: each row names two different experts. Among the 128 rows of one device (aligned blocks of rows), no expert is named more than 10 times, and in every draw some expert is named exactly 10 times by the rows of some device.
All inputs are finite; a program needn't handle non-finite values.
Results may differ from a plain program's by a relative error of at most 0.012.
Values may be sent and summed in bfloat16 or wider, within the bound.
No kernel may reach another device: no remote copies, remote signals or barrier semaphores. Data moves between devices by JAX's collectives and lax.ppermute only.
A program may use at most 128 MiB of HBM per device.

v0:
```python
import functools

import jax
import jax.numpy as jnp
from jax import lax
from jax.experimental import pallas as pl
from jax.experimental.pallas import tpu as pltpu
from jax.sharding import PartitionSpec as P


epsilon = 1e-06
bf16 = jnp.bfloat16
f32 = jnp.float32

CHUNKS = ((8, 2),)
STEPS = 4


def layout(features):
    chunks, first = [], 0
    for sizes in CHUNKS:
        parts, lane = [], 0
        for size in sizes:
            parts.append((size, first, lane, size * features // 8))
            first += size
            lane += size * features // 8
        chunks.append((tuple(parts), lane))
    return chunks


def dot(a, b):
    return jnp.dot(a, b, preferred_element_type=f32)


def dot_t(a, b):
    return lax.dot_general(a, b, (((0,), (0,)), ((), ())), preferred_element_type=f32)


def iota(shape, dim):
    return lax.broadcasted_iota(jnp.int32, shape, dim)


def normalize(values, gain):
    return values * lax.rsqrt(jnp.mean(values * values, axis=-1, keepdims=True) + epsilon) * gain


def ranks(experts, routes_ref):
    tokens = routes_ref.shape[1]
    first, second = routes_ref[0:1, :], routes_ref[1:2, :]
    names = iota((experts, tokens), 0)
    hot = [(names == chosen).astype(f32) for chosen in (first, second)]
    before = (iota((tokens, tokens), 0) < iota((tokens, tokens), 1)).astype(bf16)
    ahead = [dot(h.astype(bf16), before) for h in hot]
    ahead[1] = ahead[1] + jnp.sum(hot[0], axis=1, keepdims=True)
    rank = [jnp.sum(h * a, axis=0, keepdims=True).astype(jnp.int32) for h, a in zip(hot, ahead)]
    return (first, second), rank


def places(experts, tokens, chosen, rank, part, j):
    size, first, _, _ = part
    rows = iota((experts * 8, tokens), 0)
    found = []
    for e, r in zip(chosen, rank):
        inside = (r >= first) & (r < first + size)
        found.append(rows == jnp.where(inside, e * 8 + j * size + r - first, -1))
    return found


def pack_kernel(chunks, routes_ref, rows_ref, gain_ref, *wire_refs):
    experts = wire_refs[0].shape[0] // 8
    tokens = routes_ref.shape[1]
    normed = normalize(rows_ref[...].astype(f32), gain_ref[...]).astype(bf16)
    chosen, rank = ranks(experts, routes_ref)
    for (parts, _), wire_ref in zip(chunks, wire_refs):
        for part in parts:
            _, _, lane, width = part
            total = None
            for j in range(normed.shape[1] // width):
                found = places(experts, tokens, chosen, rank, part, j)
                taken = dot((found[0] | found[1]).astype(f32).astype(bf16), normed[:, j * width : (j + 1) * width])
                total = taken if total is None else total + taken
            wire_ref[:, lane : lane + width] = total.astype(bf16)


def combine_kernel(chunks, routes_ref, weight_ref, gain_ref, *refs):
    wire_refs, out_ref, total = refs[:-2], refs[-2], refs[-1]
    experts = wire_refs[0].shape[0] // 8
    tokens = routes_ref.shape[1]
    features = out_ref.shape[1]
    chosen, rank = ranks(experts, routes_ref)
    weights = (weight_ref[0:1, :], weight_ref[1:2, :])
    total[...] = jnp.zeros_like(total)
    for (parts, _), wire_ref in zip(chunks, wire_refs):
        for part in parts:
            _, _, lane, width = part
            for j in range(features // width):
                found = places(experts, tokens, chosen, rank, part, j)
                scale = jnp.where(found[0], weights[0], 0.0) + jnp.where(found[1], weights[1], 0.0)
                high = scale.astype(bf16)
                low = (scale - high.astype(f32)).astype(bf16)
                held = wire_ref[:, lane : lane + width]
                total[:, j * width : (j + 1) * width] += dot_t(high, held) + dot_t(low, held)
    out_ref[...] = normalize(total[...], gain_ref[...]).astype(out_ref.dtype)


def expert_kernel(parts, count, *refs):
    wires, (gate_ref, up_ref, down_ref) = refs[:count], refs[count : count + 3]
    outs = refs[count + 3 : 2 * count + 3]
    rows_ref, hidden_ref, result_ref, gate_sum, up_sum, gate_buf, up_buf, down_buf, sems = refs[2 * count + 3 :]
    features, hidden = gate_ref.shape
    deep = features // STEPS
    wide = 512

    def fetch(source, target, length, k, sem):
        rows = pl.ds(k * length, length)
        return pltpu.make_async_copy(source.at[rows], target.at[rows], sem)

    gate_copies = [fetch(gate_ref, gate_buf, deep, k, sems.at[k]) for k in range(STEPS)]
    up_copies = [fetch(up_ref, up_buf, deep, k, sems.at[STEPS + k]) for k in range(STEPS)]
    down_copies = [fetch(down_ref, down_buf, hidden // 2, k, sems.at[2 * STEPS + k]) for k in range(2)]
    for gate_copy, up_copy in zip(gate_copies, up_copies):
        gate_copy.start()
        up_copy.start()
    for down_copy in down_copies:
        down_copy.start()

    places_of = []
    base = 0
    for wire in wires:
        experts = wire.shape[0] // 8
        for size, _, lane, width in parts:
            length = experts * size
            places_of.append((wire, base, length, size, lane, width))
            base += length

    def picking(length, size, j, across):
        shape = (length * 8 // size, length) if across else (length, length * 8 // size)
        row, place = iota(shape, 1 if across else 0), iota(shape, 0 if across else 1)
        return (place == row // size * 8 + j * size + row % size).astype(f32).astype(bf16)

    for wire, start, length, size, lane, width in places_of:
        for j in range(8 // size):
            held = wire[:, lane : lane + width]
            if size < 8:
                held = dot(picking(length, size, j, False), held).astype(bf16)
            rows_ref[start : start + length, j * width : (j + 1) * width] = held

    for k in range(STEPS):
        gate_copies[k].wait()
        up_copies[k].wait()
        held = rows_ref[:, k * deep : (k + 1) * deep]
        for start in range(0, hidden, wide):
            cols = slice(start, min(start + wide, hidden))
            gate = dot(held, gate_buf[k * deep : (k + 1) * deep, cols])
            up = dot(held, up_buf[k * deep : (k + 1) * deep, cols])
            if k > 0:
                gate, up = gate_sum[:, cols] + gate, up_sum[:, cols] + up
            if k < STEPS - 1:
                gate_sum[:, cols], up_sum[:, cols] = gate, up
            else:
                hidden_ref[:, cols] = (gate / (1.0 + jnp.exp(-gate)) * up).astype(bf16)
    for down_copy in down_copies:
        down_copy.wait()

    def second(i, carry):
        cols = pl.ds(pl.multiple_of(i * wide, wide), wide)
        result_ref[:, cols] = dot(hidden_ref[...], down_buf[:, cols]).astype(bf16)
        return carry

    lax.fori_loop(0, features // wide, second, 0)

    for (wire, start, length, size, lane, width), out in zip(
        places_of, [out for out in outs for _ in parts]
    ):
        total = None
        for j in range(8 // size):
            held = result_ref[start : start + length, j * width : (j + 1) * width]
            if size < 8:
                held = dot(picking(length, size, j, True), held)
            total = held if total is None else total + held
        out[:, lane : lane + width] = total.astype(bf16)


def vmem(count):
    return [pl.BlockSpec(memory_space=pltpu.VMEM)] * count


def expert_block(parts, wires, w_gate, w_up, w_down):
    features, hidden = w_gate.shape
    slots = sum(part[0] for part in parts)
    rows = sum(wire.shape[0] // 8 * slots for wire in wires)
    return pl.pallas_call(
        functools.partial(expert_kernel, parts, len(wires)),
        out_shape=[jax.ShapeDtypeStruct(wire.shape, bf16) for wire in wires],
        in_specs=vmem(len(wires)) + [pl.BlockSpec(memory_space=pl.ANY)] * 3,
        out_specs=vmem(len(wires)),
        scratch_shapes=[
            pltpu.VMEM((rows, features), bf16),
            pltpu.VMEM((rows, hidden), bf16),
            pltpu.VMEM((rows, features), bf16),
            pltpu.VMEM((rows, hidden), f32),
            pltpu.VMEM((rows, hidden), f32),
            pltpu.VMEM((features, hidden), bf16),
            pltpu.VMEM((features, hidden), bf16),
            pltpu.VMEM((hidden, features), bf16),
            pltpu.SemaphoreType.DMA((2 * STEPS + 2,)),
        ],
        compiler_params=pltpu.CompilerParams(vmem_limit_bytes=54 * 2**20),
        cost_estimate=pl.CostEstimate(
            flops=6 * rows * features * hidden,
            bytes_accessed=6 * features * hidden + 4 * rows * features,
            transcendentals=rows * hidden,
        ),
        name="experts",
    )(*wires, w_gate, w_up, w_down)


def ring(step):
    count = lax.axis_size("tp")
    return [(t, (t + step) % count) for t in range(count)]


def rightward(value):
    return lax.ppermute(value, "tp", ring(1))


def leftward(value):
    return lax.ppermute(value, "tp", ring(-1))


def added(*values):
    return sum(value.astype(f32) for value in values).astype(bf16)


def exchange(wire):
    experts = lax.axis_size("ep")
    blocks = wire.reshape(experts, 8, wire.shape[1])
    return lax.all_to_all(blocks, "ep", split_axis=0, concat_axis=0, tiled=True).reshape(wire.shape)


def routed_experts(ffn_in, ffn_gain, routes, route_weight, w_gate, w_up, w_down, out_gain):
    tokens, features = ffn_in.shape
    experts = lax.axis_size("ep")
    chunks = layout(features)
    routes_t, weight_t = routes.T, route_weight.T
    wires = pl.pallas_call(
        functools.partial(pack_kernel, chunks),
        out_shape=[jax.ShapeDtypeStruct((experts * 8, width), bf16) for _, width in chunks],
        in_specs=vmem(3),
        out_specs=vmem(len(chunks)),
        compiler_params=pltpu.CompilerParams(vmem_limit_bytes=8 * 2**20),
        cost_estimate=pl.CostEstimate(flops=2**30, bytes_accessed=2**21, transcendentals=0),
        name="pack",
    )(routes_t, ffn_in, ffn_gain[None])
    ((parts, _),) = chunks
    (wire,) = wires
    compute = functools.partial(expert_block, parts, w_gate=w_gate[0], w_up=w_up[0], w_down=w_down[0])
    own = exchange(wire)
    half = own.shape[0] // 2
    left_a, right_b = rightward(own[:half]), leftward(own[half:])
    left_b, right_a = rightward(own[half:]), leftward(own[:half])
    far_a, far_b = rightward(left_a), leftward(right_b)
    (own,) = compute([own])
    left_a, right_b = compute([left_a, right_b])
    left_b, right_a = compute([left_b, right_a])
    far_a, far_b = compute([far_a, far_b])
    from_right_b, from_left_a = leftward(left_b), rightward(right_a)
    far_a, far_b = leftward(far_a), rightward(far_b)
    from_right_a, from_left_b = leftward(added(left_a, far_a)), rightward(added(right_b, far_b))
    total = jnp.concatenate([added(own[:half], from_left_a, from_right_a), added(own[half:], from_right_b, from_left_b)])
    returned = [exchange(total)]
    return pl.pallas_call(
        functools.partial(combine_kernel, chunks),
        out_shape=jax.ShapeDtypeStruct(ffn_in.shape, bf16),
        in_specs=vmem(3 + len(chunks)),
        out_specs=pl.BlockSpec(memory_space=pltpu.VMEM),
        scratch_shapes=[pltpu.VMEM((tokens, features), f32)],
        compiler_params=pltpu.CompilerParams(vmem_limit_bytes=8 * 2**20),
        cost_estimate=pl.CostEstimate(flops=2**30, bytes_accessed=2**21, transcendentals=0),
        name="combine",
    )(routes_t, weight_t, out_gain[None], *returned)


def pool_mixer(pool_in, pool_map, pool_scale, w_out, mix_gain):
    own_rows, channels = pool_in.shape
    group_count, group_width = pool_map.shape[0], pool_map.shape[1]
    axes = ("ep", "tp")
    count = lax.axis_size(axes)
    previous = lax.ppermute(pool_in[own_rows - 16 :], axes, [(d, d + 1) for d in range(count - 1)])
    running = jnp.concatenate([previous, pool_in], axis=0).astype(f32)
    window_parts = []
    stride = 1
    for step_index in range(group_count):
        running = running[stride:] + running[:-stride]
        stride = stride * 2
        window_parts.append(running[-own_rows:, step_index * group_width : (step_index + 1) * group_width])
    windows = jnp.concatenate(window_parts, axis=1)
    offset = lax.axis_index(axes) * own_rows
    position = (offset + jnp.arange(own_rows, dtype=jnp.int32)).astype(f32)
    reaches = (2 ** (1 + jnp.arange(channels, dtype=jnp.int32) // group_width)).astype(f32)
    counts = jnp.minimum(position[:, None] + 1.0, reaches[None, :])
    contrast = (windows / counts - pool_in.astype(f32)).astype(bf16)
    mapped = jnp.einsum(
        "rgc,gcd->rgd",
        contrast.reshape(own_rows, group_count, group_width),
        pool_map,
        preferred_element_type=f32,
    ).reshape(own_rows, channels)
    pooled = (mapped * pool_scale).astype(bf16)
    projected = jnp.dot(pooled, w_out, preferred_element_type=f32)
    return normalize(projected, mix_gain).astype(bf16)


def shards(
    pool_in,
    pool_map,
    pool_scale,
    w_out,
    mix_gain,
    ffn_in,
    ffn_gain,
    routes,
    route_weight,
    w_gate,
    w_up,
    w_down,
    out_gain,
):
    mixer_out = pool_mixer(pool_in, pool_map, pool_scale, w_out, mix_gain)
    moe_out = routed_experts(ffn_in, ffn_gain, routes, route_weight, w_gate, w_up, w_down, out_gain)
    return (mixer_out, moe_out)


def solution(mesh):
    return jax.shard_map(
        shards,
        mesh=mesh,
        in_specs=(
            P(("ep", "tp"), None),
            P(),
            P(),
            P(),
            P(),
            P(("ep", "tp"), None),
            P(),
            P(("ep", "tp"), None),
            P(("ep", "tp"), None),
            P("ep", None, "tp"),
            P("ep", None, "tp"),
            P("ep", "tp", None),
            P(),
        ),
        out_specs=(P(("ep", "tp"), None), P(("ep", "tp"), None)),
        check_vma=False,
    )
```

profile of v0, /device:TPU:0, one launch (start us, length us, event | category | flops | bytes accessed | tf_op | source)
XLA Modules:
  0.0 175.1 jit_solution(3174631855588480532)
XLA Ops:
  0.7 1.1 copy-done.1
  1.7 0.7 copy-done.2
  2.4 0.7 copy-done.4
  3.1 2.0 %pack.1 = bf16[256,2560]{1,0:T(8,128)(2,1)} custom-call(s32[2,128]{1,0:T(2,128)S(1)} %bitcast.32, bf16[128,2048]{1,0:T(8,128)(2,1)S(1)} %copy-done.1, f32[1,2048]{1,0:T(1,128)S(1)} %bitcast.30), custom_call_target="tpu_custom_call" | custom-call | flops 1073741824 | bytes 2097152 | tf_op jit(solution)/shard_map/pack/pallas_call | solution.py:246
  5.1 8.6 %all-to-all-start = ((bf16[32,8,2560]{2,1,0:T(8,128)(2,1)}), bf16[32,8,2560]{2,1,0:T(8,128)(2,1)S(1)}, u32[]{:S(2)}, u32[]{:S(2)}) async-start(bf16[32,8,2560]{2,1,0:T(8,128)(2,1)} %bitcast.6), calls=%async_computation | async-start | bytes 2621440 | tf_op jit(solution)/shard_map/all_to_all | solution.py:238
  13.7 3.4 %collective-permute-start = (bf16[16,1024]{1,0:T(8,128)(2,1)S(1)}, bf16[16,1024]{1,0:T(8,128)(2,1)S(1)}, u32[]{:S(2)}, u32[]{:S(2)}) collective-permute-start(bf16[16,1024]{1,0:T(8,128)(2,1)S(1)} %slice.59), channel_id=1, source_target_pairs={{0,1},{1,2},{2,3},{3,4},{4,5},{5,6},{6,7},{7,8},{8,9},{9,10},{10,1... | collective-permute-start | bytes 98312 | tf_op jit(solution)/shard_map/ppermute | solution.py:289
  17.2 1.5 collective-permute-done
  18.7 0.1 maximum_convert_fusion
  18.8 15.6 %all-to-all-done = bf16[32,8,2560]{2,1,0:T(8,128)(2,1)S(1)} async-done(((bf16[32,8,2560]{2,1,0:T(8,128)(2,1)}), bf16[32,8,2560]{2,1,0:T(8,128)(2,1)S(1)}, u32[]{:S(2)}, u32[]{:S(2)}) %all-to-all-start) | async-done | bytes 1310752 | tf_op jit(solution)/shard_map/all_to_all | solution.py:238
  34.5 0.1 slice_bitcast_fusion.1
  34.6 1.0 copy-done.7
  35.6 1.3 collective-permute-start.4
  36.8 2.0 %collective-permute-start.5 = (bf16[128,2560]{1,0:T(8,128)(2,1)S(1)}, bf16[128,2560]{1,0:T(8,128)(2,1)S(1)}, u32[]{:S(2)}, u32[]{:S(2)}) collective-permute-start(bf16[128,2560]{1,0:T(8,128)(2,1)S(1)} %get-tuple-element.16), channel_id=1, source_target_pairs={{0,3},{1,0},{2,1},{3,2},{4,7},{5,4},{6,5},{7,6},{8,11},{9,8},{10,9... | collective-permute-start | bytes 1966088 | tf_op jit(solution)/shard_map/ppermute | solution.py:228
  38.8 0.1 slice_add_fusion.2
  38.9 0.2 slice_add_fusion.1
  39.1 0.2 slice_add_fusion
  39.3 12.8 %collective-permute-done.4.refs_0_ = bf16[128,2560]{1,0:T(8,128)(2,1)S(1)} collective-permute-done((bf16[128,2560]{1,0:T(8,128)(2,1)S(1)}, bf16[128,2560]{1,0:T(8,128)(2,1)S(1)}, u32[]{:S(2)}, u32[]{:S(2)}) %collective-permute-start.4) | collective-permute-done | bytes 655392 | tf_op jit(solution)/shard_map/ppermute | solution.py:224
  52.1 0.4 collective-permute-start.6
  52.5 2.9 %collective-permute-start.7 = (bf16[128,2560]{1,0:T(8,128)(2,1)S(1)}, bf16[128,2560]{1,0:T(8,128)(2,1)S(1)}, u32[]{:S(2)}, u32[]{:S(2)}) collective-permute-start(bf16[128,2560]{1,0:T(8,128)(2,1)S(1)} %collective-permute-done.5.refs_1_), channel_id=1, source_target_pairs={{0,3},{1,0},{2,1},{3,2},{4,7},{5,4},{6,5},{7,6},{8,11},{9,8},{10,9... | collective-permute-start | bytes 1966088 | tf_op jit(solution)/shard_map/ppermute | solution.py:228
  55.3 0.3 fusion.21
  55.8 0.1 collective-permute-start.1
  55.9 3.2 %collective-permute-start.2 = (bf16[128,2560]{1,0:T(8,128)(2,1)S(1)}, bf16[128,2560]{1,0:T(8,128)(2,1)S(1)}, u32[]{:S(2)}, u32[]{:S(2)}) collective-permute-start(bf16[128,2560]{1,0:T(8,128)(2,1)S(1)} %get-tuple-element.17), channel_id=1, source_target_pairs={{0,3},{1,0},{2,1},{3,2},{4,7},{5,4},{6,5},{7,6},{8,11},{9,8},{10,9... | collective-permute-start | bytes 1966088 | tf_op jit(solution)/shard_map/ppermute | solution.py:228
  59.1 0.3 fusion.1
  59.4 11.5 %collective-permute-done.6.refs_0_ = bf16[128,2560]{1,0:T(8,128)(2,1)S(1)} collective-permute-done((bf16[128,2560]{1,0:T(8,128)(2,1)S(1)}, bf16[128,2560]{1,0:T(8,128)(2,1)S(1)}, u32[]{:S(2)}, u32[]{:S(2)}) %collective-permute-start.6) | collective-permute-done | bytes 655392 | tf_op jit(solution)/shard_map/ppermute | solution.py:224
  70.9 0.8 copy-done.15
  71.7 0.2 copy-done.16
  72.0 12.1 %experts.7 = (bf16[128,2560]{1,0:T(8,128)(2,1)}, bf16[128,2560]{1,0:T(8,128)(2,1)}) custom-call(bf16[128,2560]{1,0:T(8,128)(2,1)} %copy-done.15, bf16[128,2560]{1,0:T(8,128)(2,1)} %copy-done.16, bf16[2048,1408]{1,0:T(8,128)(2,1)} %bitcast.37, bf16[2048,1408]{1,0:T(8,128)(2,1)} %bitcast.41, bf16[1408,2048]{1,0:T(8,128)(2,1)} %bitcast.45), custom_call_target="tpu_custom_call" | custom-call | flops 5536481280 | bytes 19922944 | tf_op jit(solution)/shard_map/experts/pallas_call | solution.py:192
  84.0 0.7 collective-permute-start.11
  84.8 0.8 copy-done.17
  85.6 0.9 copy-done.18
  86.4 12.1 %experts.5 = (bf16[128,2560]{1,0:T(8,128)(2,1)}, bf16[128,2560]{1,0:T(8,128)(2,1)}) custom-call(bf16[128,2560]{1,0:T(8,128)(2,1)} %copy-done.17, bf16[128,2560]{1,0:T(8,128)(2,1)} %copy-done.18, bf16[2048,1408]{1,0:T(8,128)(2,1)} %bitcast.38, bf16[2048,1408]{1,0:T(8,128)(2,1)} %bitcast.42, bf16[1408,2048]{1,0:T(8,128)(2,1)} %bitcast.46), custom_call_target="tpu_custom_call" | custom-call | flops 5536481280 | bytes 19922944 | tf_op jit(solution)/shard_map/experts/pallas_call | solution.py:192
  98.5 2.9 %collective-permute-start.10 = (bf16[128,2560]{1,0:T(8,128)(2,1)}, bf16[128,2560]{1,0:T(8,128)(2,1)S(1)}, u32[]{:S(2)}, u32[]{:S(2)}) collective-permute-start(bf16[128,2560]{1,0:T(8,128)(2,1)} %get-tuple-element.11), channel_id=1, source_target_pairs={{0,3},{1,0},{2,1},{3,2},{4,7},{5,4},{6,5},{7,6},{8,11},{9,8},{10,9... | collective-permute-start | bytes 1966088 | tf_op jit(solution)/shard_map/ppermute | solution.py:228
  101.4 12.1 %experts.6 = (bf16[128,2560]{1,0:T(8,128)(2,1)}, bf16[128,2560]{1,0:T(8,128)(2,1)}) custom-call(bf16[128,2560]{1,0:T(8,128)(2,1)} %copy-done.12, bf16[128,2560]{1,0:T(8,128)(2,1)} %copy-done.13, bf16[2048,1408]{1,0:T(8,128)(2,1)} %bitcast.39, bf16[2048,1408]{1,0:T(8,128)(2,1)} %bitcast.43, bf16[1408,2048]{1,0:T(8,128)(2,1)} %bitcast.47), custom_call_target="tpu_custom_call" | custom-call | flops 5536481280 | bytes 19922944 | tf_op jit(solution)/shard_map/experts/pallas_call | solution.py:192
  113.5 3.2 %collective-permute-start.8 = (bf16[128,2560]{1,0:T(8,128)(2,1)S(1)}, bf16[128,2560]{1,0:T(8,128)(2,1)S(1)}, u32[]{:S(2)}, u32[]{:S(2)}) collective-permute-start(bf16[128,2560]{1,0:T(8,128)(2,1)S(1)} %copy-done.14), channel_id=1, source_target_pairs={{0,3},{1,0},{2,1},{3,2},{4,7},{5,4},{6,5},{7,6},{8,11},{9,8},{10,9... | collective-permute-start | bytes 1966088 | tf_op jit(solution)/shard_map/ppermute | solution.py:228
  116.8 1.2 add_convert_fusion.1
  118.1 10.7 %collective-permute-done.8 = bf16[128,2560]{1,0:T(8,128)(2,1)S(1)} collective-permute-done((bf16[128,2560]{1,0:T(8,128)(2,1)S(1)}, bf16[128,2560]{1,0:T(8,128)(2,1)S(1)}, u32[]{:S(2)}, u32[]{:S(2)}) %collective-permute-start.8) | collective-permute-done | bytes 655392 | tf_op jit(solution)/shard_map/ppermute | solution.py:228
  128.8 0.2 add_convert_fusion.3
  128.9 4.0 %collective-permute-start.9 = (bf16[128,2560]{1,0:T(8,128)(2,1)S(1)}, bf16[128,2560]{1,0:T(8,128)(2,1)S(1)}, u32[]{:S(2)}, u32[]{:S(2)}) collective-permute-start(bf16[128,2560]{1,0:T(8,128)(2,1)S(1)} %add_convert_fusion.3), channel_id=1, source_target_pairs={{0,3},{1,0},{2,1},{3,2},{4,7},{5,4},{6,5},{7,6},{8,11},{9,8},{10,9... | collective-permute-start | bytes 1966088 | tf_op jit(solution)/shard_map/ppermute | solution.py:228
  132.9 0.3 fusion.3
  133.3 12.2 %experts.4 = bf16[256,2560]{1,0:T(8,128)(2,1)} custom-call(bf16[256,2560]{1,0:T(8,128)(2,1)} %bitcast.35, bf16[2048,1408]{1,0:T(8,128)(2,1)} %bitcast.40, bf16[2048,1408]{1,0:T(8,128)(2,1)} %bitcast.44, bf16[1408,2048]{1,0:T(8,128)(2,1)} %bitcast.48), custom_call_target="tpu_custom_call" | custom-call | flops 5536481280 | bytes 19922944 | tf_op jit(solution)/shard_map/experts/pallas_call | solution.py:192
  145.5 1.8 %add_convert_fusion.2 = (bf16[128,2560]{1,0:T(8,128)(2,1)S(1)}, bf16[128,2560]{1,0:T(8,128)(2,1)S(1)}) fusion(bf16[128,2560]{1,0:T(8,128)(2,1)S(1)} %collective-permute-done.9, bf16[128,2560]{1,0:T(8,128)(2,1)S(1)} %collective-permute-done.3, bf16[256,2560]{1,0:T(8,128)(2,1)} %experts.4, bf16[128,2560]{1,0:T(8,128)(2,1)S(1)} %collective-permute-done.12, ...), kind=kLoop, calls=%fused_computation.5 | loop fusion | flops 3932160 | bytes 5242880 | tf_op jit(solution)/shard_map/convert_element_type | solution.py:232
  147.3 1.2 maximum_bitcast_fusion
  148.5 4.2 %all-to-all-start.1 = ((bf16[32,8,2560]{2,1,0:T(8,128)(2,1)}), bf16[32,8,2560]{2,1,0:T(8,128)(2,1)S(1)}, u32[]{:S(2)}, u32[]{:S(2)}) async-start(bf16[32,8,2560]{2,1,0:T(8,128)(2,1)} %maximum_bitcast_fusion), calls=%async_computation.1 | async-start | bytes 2621440 | tf_op jit(solution)/shard_map/all_to_all | solution.py:238
  152.7 0.2 fusion.2
  152.9 3.5 %multiply_reduce_fusion = (f32[256]{0:T(256)S(1)}, f32[256,2048]{1,0:T(8,128)S(1)}) fusion(bf16[256,1024]{0,1:T(8,128)(2,1)S(1)} %fusion.2, bf16[1024,2048]{1,0:T(8,128)(2,1)} %param.16), kind=kOutput, calls=%fused_computation.1 | convolution fusion | flops 1074790144 | bytes 6816768 | tf_op jit(solution)/shard_map/dot_general | solution.py:310
  156.5 1.2 multiply_convert_fusion
  157.7 15.5 %all-to-all-done.1 = bf16[32,8,2560]{2,1,0:T(8,128)(2,1)S(1)} async-done(((bf16[32,8,2560]{2,1,0:T(8,128)(2,1)}), bf16[32,8,2560]{2,1,0:T(8,128)(2,1)S(1)}, u32[]{:S(2)}, u32[]{:S(2)}) %all-to-all-start.1) | async-done | bytes 1310752 | tf_op jit(solution)/shard_map/all_to_all | solution.py:238
  173.2 1.9 %combine.1 = bf16[128,2048]{1,0:T(8,128)(2,1)} custom-call(s32[2,128]{1,0:T(2,128)S(1)} %bitcast.33, f32[2,128]{1,0:T(2,128)S(1)} %bitcast.34, f32[1,2048]{1,0:T(1,128)S(1)} %bitcast.31, bf16[256,2560]{1,0:T(8,128)(2,1)S(1)} %bitcast.29), custom_call_target="tpu_custom_call" | custom-call | flops 1073741824 | bytes 2097152 | tf_op jit(solution)/shard_map/combine/pallas_call | solution.py:272
  (49 shorter events, 0.4 us)
Async XLA Ops:
  0.6 132.3 %copy-start = (bf16[4,256,256]{2,1,0:T(8,128)(2,1)S(1)}, bf16[4,256,256]{2,1,0:T(8,128)(2,1)}, u32[]{:S(2)}) copy-start(bf16[4,256,256]{2,1,0:T(8,128)(2,1)} %param.14) | copy-start | bytes 1572868
  0.6 1.1 copy-start.1
  1.7 0.7 copy-start.2
  2.4 0.7 copy-start.4
  5.1 8.6 %copy-start.8 = (bf16[256,1024]{1,0:T(8,128)(2,1)S(1)}, bf16[256,1024]{1,0:T(8,128)(2,1)}, u32[]{:S(2)}) copy-start(bf16[256,1024]{1,0:T(8,128)(2,1)} %param.13) | copy-start | bytes 1572868
  5.1 29.4 %all-to-all-start = ((bf16[32,8,2560]{2,1,0:T(8,128)(2,1)}), bf16[32,8,2560]{2,1,0:T(8,128)(2,1)S(1)}, u32[]{:S(2)}, u32[]{:S(2)}) async-start(bf16[32,8,2560]{2,1,0:T(8,128)(2,1)} %bitcast.6), calls=%async_computation | async-start | bytes 2621440 | tf_op jit(solution)/shard_map/all_to_all | solution.py:238
  13.7 5.0 %collective-permute-start = (bf16[16,1024]{1,0:T(8,128)(2,1)S(1)}, bf16[16,1024]{1,0:T(8,128)(2,1)S(1)}, u32[]{:S(2)}, u32[]{:S(2)}) collective-permute-start(bf16[16,1024]{1,0:T(8,128)(2,1)S(1)} %slice.59), channel_id=1, source_target_pairs={{0,1},{1,2},{2,3},{3,4},{4,5},{5,6},{6,7},{7,8},{8,9},{9,10},{10,1... | collective-permute-start | bytes 98312 | tf_op jit(solution)/shard_map/ppermute | solution.py:289
  34.5 1.1 copy-start.7
  35.6 16.5 %collective-permute-start.4 = (bf16[128,2560]{1,0:T(8,128)(2,1)S(1)}, bf16[128,2560]{1,0:T(8,128)(2,1)S(1)}, u32[]{:S(2)}, u32[]{:S(2)}) collective-permute-start(bf16[128,2560]{1,0:T(8,128)(2,1)S(1)} %get-tuple-element.17), channel_id=1, source_target_pairs={{0,1},{1,2},{2,3},{3,0},{4,5},{5,6},{6,7},{7,4},{8,9},{9,10},{10,1... | collective-permute-start | bytes 1966088 | tf_op jit(solution)/shard_map/ppermute | solution.py:224
  36.8 15.6 %collective-permute-start.5 = (bf16[128,2560]{1,0:T(8,128)(2,1)S(1)}, bf16[128,2560]{1,0:T(8,128)(2,1)S(1)}, u32[]{:S(2)}, u32[]{:S(2)}) collective-permute-start(bf16[128,2560]{1,0:T(8,128)(2,1)S(1)} %get-tuple-element.16), channel_id=1, source_target_pairs={{0,3},{1,0},{2,1},{3,2},{4,7},{5,4},{6,5},{7,6},{8,11},{9,8},{10,9... | collective-permute-start | bytes 1966088 | tf_op jit(solution)/shard_map/ppermute | solution.py:228
  52.1 3.5 %copy-start.12 = (bf16[128,2560]{1,0:T(8,128)(2,1)}, bf16[128,2560]{1,0:T(8,128)(2,1)S(1)}, u32[]{:S(2)}) copy-start(bf16[128,2560]{1,0:T(8,128)(2,1)S(1)} %collective-permute-done.4.refs_0_) | copy-start | bytes 1966084
  52.1 18.8 %collective-permute-start.6 = (bf16[128,2560]{1,0:T(8,128)(2,1)S(1)}, bf16[128,2560]{1,0:T(8,128)(2,1)S(1)}, u32[]{:S(2)}, u32[]{:S(2)}) collective-permute-start(bf16[128,2560]{1,0:T(8,128)(2,1)S(1)} %collective-permute-done.4.refs_0_), channel_id=1, source_target_pairs={{0,1},{1,2},{2,3},{3,0},{4,5},{5,6},{6,7},{7,4},{8,9},{9,10},{10,1... | collective-permute-start | bytes 1966088 | tf_op jit(solution)/shard_map/ppermute | solution.py:224
  52.5 3.2 %copy-start.13 = (bf16[128,2560]{1,0:T(8,128)(2,1)}, bf16[128,2560]{1,0:T(8,128)(2,1)S(1)}, u32[]{:S(2)}) copy-start(bf16[128,2560]{1,0:T(8,128)(2,1)S(1)} %collective-permute-done.5.refs_1_) | copy-start | bytes 1966084
  52.5 18.4 %collective-permute-start.7 = (bf16[128,2560]{1,0:T(8,128)(2,1)S(1)}, bf16[128,2560]{1,0:T(8,128)(2,1)S(1)}, u32[]{:S(2)}, u32[]{:S(2)}) collective-permute-start(bf16[128,2560]{1,0:T(8,128)(2,1)S(1)} %collective-permute-done.5.refs_1_), channel_id=1, source_target_pairs={{0,3},{1,0},{2,1},{3,2},{4,7},{5,4},{6,5},{7,6},{8,11},{9,8},{10,9... | collective-permute-start | bytes 1966088 | tf_op jit(solution)/shard_map/ppermute | solution.py:228
  55.8 28.9 %collective-permute-start.1 = (bf16[128,2560]{1,0:T(8,128)(2,1)S(1)}, bf16[128,2560]{1,0:T(8,128)(2,1)S(1)}, u32[]{:S(2)}, u32[]{:S(2)}) collective-permute-start(bf16[128,2560]{1,0:T(8,128)(2,1)S(1)} %get-tuple-element.16), channel_id=1, source_target_pairs={{0,1},{1,2},{2,3},{3,0},{4,5},{5,6},{6,7},{7,4},{8,9},{9,10},{10,1... | collective-permute-start | bytes 1966088 | tf_op jit(solution)/shard_map/ppermute | solution.py:224
  55.9 28.9 %collective-permute-start.2 = (bf16[128,2560]{1,0:T(8,128)(2,1)S(1)}, bf16[128,2560]{1,0:T(8,128)(2,1)S(1)}, u32[]{:S(2)}, u32[]{:S(2)}) collective-permute-start(bf16[128,2560]{1,0:T(8,128)(2,1)S(1)} %get-tuple-element.17), channel_id=1, source_target_pairs={{0,3},{1,0},{2,1},{3,2},{4,7},{5,4},{6,5},{7,6},{8,11},{9,8},{10,9... | collective-permute-start | bytes 1966088 | tf_op jit(solution)/shard_map/ppermute | solution.py:228
  70.9 0.8 copy-start.15
  70.9 1.0 copy-start.16
  84.0 32.7 %collective-permute-start.11 = (bf16[128,2560]{1,0:T(8,128)(2,1)}, bf16[128,2560]{1,0:T(8,128)(2,1)S(1)}, u32[]{:S(2)}, u32[]{:S(2)}) collective-permute-start(bf16[128,2560]{1,0:T(8,128)(2,1)} %get-tuple-element.13), channel_id=1, source_target_pairs={{0,1},{1,2},{2,3},{3,0},{4,5},{5,6},{6,7},{7,4},{8,9},{9,10},{10,1... | collective-permute-start | bytes 1966088 | tf_op jit(solution)/shard_map/ppermute | solution.py:224
  84.8 0.8 copy-start.17
  85.6 0.9 copy-start.18
  98.5 47.0 %collective-permute-start.10 = (bf16[128,2560]{1,0:T(8,128)(2,1)}, bf16[128,2560]{1,0:T(8,128)(2,1)S(1)}, u32[]{:S(2)}, u32[]{:S(2)}) collective-permute-start(bf16[128,2560]{1,0:T(8,128)(2,1)} %get-tuple-element.11), channel_id=1, source_target_pairs={{0,3},{1,0},{2,1},{3,2},{4,7},{5,4},{6,5},{7,6},{8,11},{9,8},{10,9... | collective-permute-start | bytes 1966088 | tf_op jit(solution)/shard_map/ppermute | solution.py:228
  101.4 12.2 %copy-start.14 = (bf16[128,2560]{1,0:T(8,128)(2,1)S(1)}, bf16[128,2560]{1,0:T(8,128)(2,1)}, u32[]{:S(2)}) copy-start(bf16[128,2560]{1,0:T(8,128)(2,1)} %get-tuple-element.10) | copy-start | bytes 1966084
  101.4 44.1 %collective-permute-start.3 = (bf16[128,2560]{1,0:T(8,128)(2,1)}, bf16[128,2560]{1,0:T(8,128)(2,1)S(1)}, u32[]{:S(2)}, u32[]{:S(2)}) collective-permute-start(bf16[128,2560]{1,0:T(8,128)(2,1)} %get-tuple-element.8), channel_id=1, source_target_pairs={{0,1},{1,2},{2,3},{3,0},{4,5},{5,6},{6,7},{7,4},{8,9},{9,10},{10,1... | collective-permute-start | bytes 1966088 | tf_op jit(solution)/shard_map/ppermute | solution.py:224
  113.5 15.3 %copy-start.9 = (bf16[128,2560]{1,0:T(8,128)(2,1)S(1)}, bf16[128,2560]{1,0:T(8,128)(2,1)}, u32[]{:S(2)}) copy-start(bf16[128,2560]{1,0:T(8,128)(2,1)} %get-tuple-element.9) | copy-start | bytes 1966084
  113.5 15.3 %collective-permute-start.8 = (bf16[128,2560]{1,0:T(8,128)(2,1)S(1)}, bf16[128,2560]{1,0:T(8,128)(2,1)S(1)}, u32[]{:S(2)}, u32[]{:S(2)}) collective-permute-start(bf16[128,2560]{1,0:T(8,128)(2,1)S(1)} %copy-done.14), channel_id=1, source_target_pairs={{0,3},{1,0},{2,1},{3,2},{4,7},{5,4},{6,5},{7,6},{8,11},{9,8},{10,9... | collective-permute-start | bytes 1966088 | tf_op jit(solution)/shard_map/ppermute | solution.py:228
  118.0 27.5 %collective-permute-start.12 = (bf16[128,2560]{1,0:T(8,128)(2,1)S(1)}, bf16[128,2560]{1,0:T(8,128)(2,1)S(1)}, u32[]{:S(2)}, u32[]{:S(2)}) collective-permute-start(bf16[128,2560]{1,0:T(8,128)(2,1)S(1)} %add_convert_fusion.1), channel_id=1, source_target_pairs={{0,1},{1,2},{2,3},{3,0},{4,5},{5,6},{6,7},{7,4},{8,9},{9,10},{10,1... | collective-permute-start | bytes 1966088 | tf_op jit(solution)/shard_map/ppermute | solution.py:224
  128.9 16.6 %collective-permute-start.9 = (bf16[128,2560]{1,0:T(8,128)(2,1)S(1)}, bf16[128,2560]{1,0:T(8,128)(2,1)S(1)}, u32[]{:S(2)}, u32[]{:S(2)}) collective-permute-start(bf16[128,2560]{1,0:T(8,128)(2,1)S(1)} %add_convert_fusion.3), channel_id=1, source_target_pairs={{0,3},{1,0},{2,1},{3,2},{4,7},{5,4},{6,5},{7,6},{8,11},{9,8},{10,9... | collective-permute-start | bytes 1966088 | tf_op jit(solution)/shard_map/ppermute | solution.py:228
  148.5 4.2 %copy-start.11 = (f32[1024]{0:T(1024)S(1)}, f32[1024]{0:T(1024)}, u32[]{:S(2)}) copy-start(f32[1024]{0:T(1024)} %param.15) | copy-start | bytes 12292
  148.5 24.8 %all-to-all-start.1 = ((bf16[32,8,2560]{2,1,0:T(8,128)(2,1)}), bf16[32,8,2560]{2,1,0:T(8,128)(2,1)S(1)}, u32[]{:S(2)}, u32[]{:S(2)}) async-start(bf16[32,8,2560]{2,1,0:T(8,128)(2,1)} %maximum_bitcast_fusion), calls=%async_computation.1 | async-start | bytes 2621440 | tf_op jit(solution)/shard_map/all_to_all | solution.py:238
  152.9 3.6 %copy-start.10 = (f32[2048]{0:T(1024)S(1)}, f32[2048]{0:T(1024)}, u32[]{:S(2)}) copy-start(f32[2048]{0:T(1024)} %param.17) | copy-start | bytes 24580
  156.5 16.8 %copy-start.3 = (f32[2048]{0:T(1024)S(1)}, f32[2048]{0:T(1024)}, u32[]{:S(2)}) copy-start(f32[2048]{0:T(1024)} %param.25) | copy-start | bytes 24580
  156.5 16.7 %copy-start.5 = (s32[128,2]{0,1:T(2,128)S(1)}, s32[128,2]{0,1:T(2,128)}, u32[]{:S(2)}) copy-start(s32[128,2]{0,1:T(2,128)} %param.20) | copy-start | bytes 3076
  156.5 16.7 %copy-start.6 = (f32[128,2]{0,1:T(2,128)S(1)}, f32[128,2]{0,1:T(2,128)}, u32[]{:S(2)}) copy-start(f32[128,2]{0,1:T(2,128)} %param.21) | copy-start | bytes 3076
where the time goes:
time: 176 us; the launch traced here: 175 us
  waiting for transfers between devices  67.6 us (38%)
  Pallas kernels  52.4 us (30%)
  starting transfers between devices  36.8 us (21%)
  other arithmetic  6.72 us (4%)
  local copies, waits for them, and re-layouts  6.7 us (4%)
  matrix products  3.89 us (2%)
    pallas_call x4, Pallas kernels, expert_block(): pl.pallas_call(functools.partial(expert_kernel, parts, len(wires)), out_s...  48.5 us
    all_to_all x2, waiting for transfers between devices, exchange(): lax.all_to_all(blocks, 'ep', split_axis=0, concat_axis=0, tiled=True)  31.1 us
    ppermute x6, waiting for transfers between devices, rightward(): return lax.ppermute(value, 'tp', ring(1))  24.3 us
    ppermute x6, starting transfers between devices, leftward(): return lax.ppermute(value, 'tp', ring(-1))  18.1 us
    all_to_all x2, starting transfers between devices, exchange(): lax.all_to_all(blocks, 'ep', split_axis=0, concat_axis=0, tiled=True)  12.8 us
    ppermute x6, waiting for transfers between devices, leftward(): return lax.ppermute(value, 'tp', ring(-1))  10.7 us
    unnamed x38, local copies, waits for them, and re-layouts  6.25 us
    dot_general x1, matrix products, pool_mixer(): projected = jnp.dot(pooled, w_out, preferred_element_type=f32)  3.55 us
  transfers between devices with their start and end apart: 15, of which 6 were waited for; matrix products, arithmetic and copies ran while one was open for 5% of the time, Pallas kernels for 28%

commit v1 on v0

--- a/solution.py
+++ b/solution.py
@@ -13,7 +13,7 @@
 f32 = jnp.float32
 
 CHUNKS = ((8, 2),)
-STEPS = 4
+LIMIT = 14
 
 
 def layout(features):
@@ -106,23 +106,9 @@
 def expert_kernel(parts, count, *refs):
     wires, (gate_ref, up_ref, down_ref) = refs[:count], refs[count : count + 3]
     outs = refs[count + 3 : 2 * count + 3]
-    rows_ref, hidden_ref, result_ref, gate_sum, up_sum, gate_buf, up_buf, down_buf, sems = refs[2 * count + 3 :]
+    rows_ref, hidden_ref, result_ref = refs[2 * count + 3 :]
     features, hidden = gate_ref.shape
-    deep = features // STEPS
     wide = 512
-
-    def fetch(source, target, length, k, sem):
-        rows = pl.ds(k * length, length)
-        return pltpu.make_async_copy(source.at[rows], target.at[rows], sem)
-
-    gate_copies = [fetch(gate_ref, gate_buf, deep, k, sems.at[k]) for k in range(STEPS)]
-    up_copies = [fetch(up_ref, up_buf, deep, k, sems.at[STEPS + k]) for k in range(STEPS)]
-    down_copies = [fetch(down_ref, down_buf, hidden // 2, k, sems.at[2 * STEPS + k]) for k in range(2)]
-    for gate_copy, up_copy in zip(gate_copies, up_copies):
-        gate_copy.start()
-        up_copy.start()
-    for down_copy in down_copies:
-        down_copy.start()
 
     places_of = []
     base = 0
@@ -145,26 +131,15 @@
                 held = dot(picking(length, size, j, False), held).astype(bf16)
             rows_ref[start : start + length, j * width : (j + 1) * width] = held
 
-    for k in range(STEPS):
-        gate_copies[k].wait()
-        up_copies[k].wait()
-        held = rows_ref[:, k * deep : (k + 1) * deep]
-        for start in range(0, hidden, wide):
-            cols = slice(start, min(start + wide, hidden))
-            gate = dot(held, gate_buf[k * deep : (k + 1) * deep, cols])
-            up = dot(held, up_buf[k * deep : (k + 1) * deep, cols])
-            if k > 0:
-                gate, up = gate_sum[:, cols] + gate, up_sum[:, cols] + up
-            if k < STEPS - 1:
-                gate_sum[:, cols], up_sum[:, cols] = gate, up
-            else:
-                hidden_ref[:, cols] = (gate / (1.0 + jnp.exp(-gate)) * up).astype(bf16)
-    for down_copy in down_copies:
-        down_copy.wait()
+    for start in range(0, hidden, wide):
+        cols = slice(start, min(start + wide, hidden))
+        gate = dot(rows_ref[...], gate_ref[:, cols])
+        up = dot(rows_ref[...], up_ref[:, cols])
+        hidden_ref[:, cols] = (gate / (1.0 + jnp.exp(-gate)) * up).astype(bf16)
 
     def second(i, carry):
         cols = pl.ds(pl.multiple_of(i * wide, wide), wide)
-        result_ref[:, cols] = dot(hidden_ref[...], down_buf[:, cols]).astype(bf16)
+        result_ref[:, cols] = dot(hidden_ref[...], down_ref[:, cols]).astype(bf16)
         return carry
 
     lax.fori_loop(0, features // wide, second, 0)
@@ -192,20 +167,14 @@
     return pl.pallas_call(
         functools.partial(expert_kernel, parts, len(wires)),
         out_shape=[jax.ShapeDtypeStruct(wire.shape, bf16) for wire in wires],
-        in_specs=vmem(len(wires)) + [pl.BlockSpec(memory_space=pl.ANY)] * 3,
+        in_specs=vmem(len(wires) + 3),
         out_specs=vmem(len(wires)),
         scratch_shapes=[
             pltpu.VMEM((rows, features), bf16),
             pltpu.VMEM((rows, hidden), bf16),
             pltpu.VMEM((rows, features), bf16),
-            pltpu.VMEM((rows, hidden), f32),
-            pltpu.VMEM((rows, hidden), f32),
-            pltpu.VMEM((features, hidden), bf16),
-            pltpu.VMEM((features, hidden), bf16),
-            pltpu.VMEM((hidden, features), bf16),
-            pltpu.SemaphoreType.DMA((2 * STEPS + 2,)),
         ],
-        compiler_params=pltpu.CompilerParams(vmem_limit_bytes=54 * 2**20),
+        compiler_params=pltpu.CompilerParams(vmem_limit_bytes=LIMIT * 2**20),
         cost_estimate=pl.CostEstimate(
             flops=6 * rows * features * hidden,
             bytes_accessed=6 * features * hidden + 4 * rows * features,

time: 176 us -> 167 us (0.949)
  Pallas kernels: 52.4 us -> 34.3 us
  starting transfers between devices: 36.8 us -> 43.4 us
  waiting for transfers between devices: 67.6 us -> 71 us
  other arithmetic: 6.72 us -> 4.33 us
    pallas_call x4, Pallas kernels: 48.5 us -> 30.4 us  [expert_block(): pl.pallas_call(functools.partial(expert_kernel, parts, len(wires)), out_s...]
    all_to_all x2, starting transfers between devices: 12.8 us -> 19.3 us  [exchange(): lax.all_to_all(blocks, 'ep', split_axis=0, concat_axis=0, tiled=True)]
    ppermute x6, waiting for transfers between devices: 10.7 us -> 13.9 us  [leftward(): return lax.ppermute(value, 'tp', ring(-1))]
    convert_element_type x3, other arithmetic: 3.15 us -> 0.77 us  [added(): return sum((value.astype(f32) for value in values)).astype(bf16)]
    unnamed x38 -> x28, local copies, waits for them, and re-layouts: 6.25 us -> 7.79 us
  transfers between devices with their start and end apart: 15 -> 15, of which waited for: 6 -> 7; matrix products, arithmetic and copies ran while one was open for 5% -> 4% of each run, Pallas kernels for 28% -> 18%
where the time goes in v1:
time: 167 us; the launch traced here: 166 us
  waiting for transfers between devices  71 us (43%)
  starting transfers between devices  43.4 us (26%)
  Pallas kernels  34.3 us (21%)
  local copies, waits for them, and re-layouts  8.1 us (5%)
  other arithmetic  4.33 us (3%)
  matrix products  3.89 us (2%)
    all_to_all x2, waiting for transfers between devices, exchange(): lax.all_to_all(blocks, 'ep', split_axis=0, concat_axis=0, tiled=True)  31.1 us
    pallas_call x4, Pallas kernels, expert_block(): pl.pallas_call(functools.partial(expert_kernel, parts, len(wires)), out_s...  30.4 us
    ppermute x6, waiting for transfers between devices, rightward(): return lax.ppermute(value, 'tp', ring(1))  24.4 us
    all_to_all x2, starting transfers between devices, exchange(): lax.all_to_all(blocks, 'ep', split_axis=0, concat_axis=0, tiled=True)  19.3 us
    ppermute x6, starting transfers between devices, leftward(): return lax.ppermute(value, 'tp', ring(-1))  17.8 us
    ppermute x6, waiting for transfers between devices, leftward(): return lax.ppermute(value, 'tp', ring(-1))  13.9 us
    unnamed x28, local copies, waits for them, and re-layouts  7.79 us
    dot_general x1, matrix products, pool_mixer(): projected = jnp.dot(pooled, w_out, preferred_element_type=f32)  3.55 us
  transfers between devices with their start and end apart: 15, of which 7 were waited for; matrix products, arithmetic and copies ran while one was open for 4% of the time, Pallas kernels for 18%

profile of v1, /device:TPU:0, one launch (start us, length us, event | category | flops | bytes accessed | tf_op | source)
XLA Modules:
  0.0 166.0 jit_solution(9568721385200642314)
XLA Ops:
  0.7 1.1 copy-done.3
  1.7 0.7 copy-done.4
  2.4 0.7 copy-done.6
  3.1 2.0 %pack.1 = bf16[256,2560]{1,0:T(8,128)(2,1)} custom-call(s32[2,128]{1,0:T(2,128)S(1)} %bitcast.47, bf16[128,2048]{1,0:T(8,128)(2,1)S(1)} %copy-done.3, f32[1,2048]{1,0:T(1,128)S(1)} %bitcast.45), custom_call_target="tpu_custom_call" | custom-call | flops 1073741824 | bytes 2097152 | tf_op jit(solution)/shard_map/pack/pallas_call | solution.py:215
  5.1 8.6 %all-to-all-start = ((bf16[32,8,2560]{2,1,0:T(8,128)(2,1)}), bf16[32,8,2560]{2,1,0:T(8,128)(2,1)S(1)}, u32[]{:S(2)}, u32[]{:S(2)}) async-start(bf16[32,8,2560]{2,1,0:T(8,128)(2,1)} %bitcast.6), calls=%async_computation | async-start | bytes 2621440 | tf_op jit(solution)/shard_map/all_to_all | solution.py:207
  13.7 3.4 %collective-permute-start = (bf16[16,1024]{1,0:T(8,128)(2,1)S(1)}, bf16[16,1024]{1,0:T(8,128)(2,1)S(1)}, u32[]{:S(2)}, u32[]{:S(2)}) collective-permute-start(bf16[16,1024]{1,0:T(8,128)(2,1)S(1)} %slice.59), channel_id=1, source_target_pairs={{0,1},{1,2},{2,3},{3,4},{4,5},{5,6},{6,7},{7,8},{8,9},{9,10},{10,1... | collective-permute-start | bytes 98312 | tf_op jit(solution)/shard_map/ppermute | solution.py:258
  17.2 1.5 collective-permute-done
  18.7 0.1 maximum_convert_fusion
  18.8 15.6 %all-to-all-done = bf16[32,8,2560]{2,1,0:T(8,128)(2,1)S(1)} async-done(((bf16[32,8,2560]{2,1,0:T(8,128)(2,1)}), bf16[32,8,2560]{2,1,0:T(8,128)(2,1)S(1)}, u32[]{:S(2)}, u32[]{:S(2)}) %all-to-all-start) | async-done | bytes 1310752 | tf_op jit(solution)/shard_map/all_to_all | solution.py:207
  34.5 0.1 slice_bitcast_fusion.1
  34.6 1.3 collective-permute-start.4
  35.9 2.0 %collective-permute-start.5 = (bf16[128,2560]{1,0:T(8,128)(2,1)S(1)}, bf16[128,2560]{1,0:T(8,128)(2,1)S(1)}, u32[]{:S(2)}, u32[]{:S(2)}) collective-permute-start(bf16[128,2560]{1,0:T(8,128)(2,1)S(1)} %get-tuple-element.16), channel_id=1, source_target_pairs={{0,3},{1,0},{2,1},{3,2},{4,7},{5,4},{6,5},{7,6},{8,11},{9,8},{10,9... | collective-permute-start | bytes 1966088 | tf_op jit(solution)/shard_map/ppermute | solution.py:197
  37.9 0.1 slice_add_fusion.2
  38.0 0.2 slice_add_fusion.1
  38.2 0.2 slice_add_fusion
  38.4 12.7 %collective-permute-done.4.refs_0_ = bf16[128,2560]{1,0:T(8,128)(2,1)S(1)} collective-permute-done((bf16[128,2560]{1,0:T(8,128)(2,1)S(1)}, bf16[128,2560]{1,0:T(8,128)(2,1)S(1)}, u32[]{:S(2)}, u32[]{:S(2)}) %collective-permute-start.4) | collective-permute-done | bytes 655392 | tf_op jit(solution)/shard_map/ppermute | solution.py:193
  51.2 0.4 collective-permute-start.6
  51.6 2.9 %collective-permute-start.7 = (bf16[128,2560]{1,0:T(8,128)(2,1)S(1)}, bf16[128,2560]{1,0:T(8,128)(2,1)S(1)}, u32[]{:S(2)}, u32[]{:S(2)}) collective-permute-start(bf16[128,2560]{1,0:T(8,128)(2,1)S(1)} %collective-permute-done.5.refs_1_), channel_id=1, source_target_pairs={{0,3},{1,0},{2,1},{3,2},{4,7},{5,4},{6,5},{7,6},{8,11},{9,8},{10,9... | collective-permute-start | bytes 1966088 | tf_op jit(solution)/shard_map/ppermute | solution.py:197
  54.4 0.1 fusion.21
  54.7 0.1 slice_add_fusion.3
  54.7 0.1 collective-permute-start.1
  54.8 3.2 %collective-permute-start.2 = (bf16[128,2560]{1,0:T(8,128)(2,1)S(1)}, bf16[128,2560]{1,0:T(8,128)(2,1)S(1)}, u32[]{:S(2)}, u32[]{:S(2)}) collective-permute-start(bf16[128,2560]{1,0:T(8,128)(2,1)S(1)} %get-tuple-element.17), channel_id=1, source_target_pairs={{0,3},{1,0},{2,1},{3,2},{4,7},{5,4},{6,5},{7,6},{8,11},{9,8},{10,9... | collective-permute-start | bytes 1966088 | tf_op jit(solution)/shard_map/ppermute | solution.py:197
  58.0 0.3 fusion.1
  58.3 11.7 %collective-permute-done.6.refs_0_ = bf16[128,2560]{1,0:T(8,128)(2,1)S(1)} collective-permute-done((bf16[128,2560]{1,0:T(8,128)(2,1)S(1)}, bf16[128,2560]{1,0:T(8,128)(2,1)S(1)}, u32[]{:S(2)}, u32[]{:S(2)}) %collective-permute-start.6) | collective-permute-done | bytes 655392 | tf_op jit(solution)/shard_map/ppermute | solution.py:193
  70.0 2.6 %copy-done.1 = bf16[1,2048,1408]{2,1,0:T(8,128)(2,1)S(1)} copy-done((bf16[1,2048,1408]{2,1,0:T(8,128)(2,1)S(1)}, bf16[1,2048,1408]{2,1,0:T(8,128)(2,1)}, u32[]{:S(2)}) %copy-start.1) | copy-done | bytes 5767192
  72.6 2.6 %copy-done.2 = bf16[1,1408,2048]{2,1,0:T(8,128)(2,1)S(1)} copy-done((bf16[1,1408,2048]{2,1,0:T(8,128)(2,1)S(1)}, bf16[1,1408,2048]{2,1,0:T(8,128)(2,1)}, u32[]{:S(2)}) %copy-start.2) | copy-done | bytes 5767192
  75.3 7.6 %experts.7 = (bf16[128,2560]{1,0:T(8,128)(2,1)S(1)}, bf16[128,2560]{1,0:T(8,128)(2,1)S(1)}) custom-call(bf16[128,2560]{1,0:T(8,128)(2,1)S(1)} %collective-permute-done.6.refs_0_, bf16[128,2560]{1,0:T(8,128)(2,1)S(1)} %collective-permute-done.7.refs_1_, bf16[2048,1408]{1,0:T(8,128)(2,1)S(1)} %bitcast.33, bf16[2048,1408]{1,0:T(8,128)(2,1)S(1)} %bitcast.37, ...), custom_call_target="tpu_custom_call" | custom-call | flops 5536481280 | bytes 19922944 | tf_op jit(solution)/shard_map/experts/pallas_call | solution.py:167
  82.9 0.9 collective-permute-start.11
  83.8 7.6 %experts.5 = (bf16[128,2560]{1,0:T(8,128)(2,1)S(1)}, bf16[128,2560]{1,0:T(8,128)(2,1)S(1)}) custom-call(bf16[128,2560]{1,0:T(8,128)(2,1)S(1)} %collective-permute-done.1.refs_0_, bf16[128,2560]{1,0:T(8,128)(2,1)S(1)} %collective-permute-done.2.refs_1_, bf16[2048,1408]{1,0:T(8,128)(2,1)S(1)} %bitcast.34, bf16[2048,1408]{1,0:T(8,128)(2,1)S(1)} %bitcast.38, ...), custom_call_target="tpu_custom_call" | custom-call | flops 5536481280 | bytes 19922944 | tf_op jit(solution)/shard_map/experts/pallas_call | solution.py:167
  91.4 2.7 %collective-permute-start.10 = (bf16[128,2560]{1,0:T(8,128)(2,1)S(1)}, bf16[128,2560]{1,0:T(8,128)(2,1)S(1)}, u32[]{:S(2)}, u32[]{:S(2)}) collective-permute-start(bf16[128,2560]{1,0:T(8,128)(2,1)S(1)} %get-tuple-element.11), channel_id=1, source_target_pairs={{0,3},{1,0},{2,1},{3,2},{4,7},{5,4},{6,5},{7,6},{8,11},{9,8},{10,9... | collective-permute-start | bytes 1966088 | tf_op jit(solution)/shard_map/ppermute | solution.py:197
  94.0 7.6 %experts.6 = (bf16[128,2560]{1,0:T(8,128)(2,1)S(1)}, bf16[128,2560]{1,0:T(8,128)(2,1)S(1)}) custom-call(bf16[128,2560]{1,0:T(8,128)(2,1)S(1)} %collective-permute-done.4.refs_0_, bf16[128,2560]{1,0:T(8,128)(2,1)S(1)} %collective-permute-done.5.refs_1_, bf16[2048,1408]{1,0:T(8,128)(2,1)S(1)} %bitcast.35, bf16[2048,1408]{1,0:T(8,128)(2,1)S(1)} %bitcast.39, ...), custom_call_target="tpu_custom_call" | custom-call | flops 5536481280 | bytes 19922944 | tf_op jit(solution)/shard_map/experts/pallas_call | solution.py:167
  101.6 3.3 %collective-permute-start.8 = (bf16[128,2560]{1,0:T(8,128)(2,1)S(1)}, bf16[128,2560]{1,0:T(8,128)(2,1)S(1)}, u32[]{:S(2)}, u32[]{:S(2)}) collective-permute-start(bf16[128,2560]{1,0:T(8,128)(2,1)S(1)} %get-tuple-element.10), channel_id=1, source_target_pairs={{0,3},{1,0},{2,1},{3,2},{4,7},{5,4},{6,5},{7,6},{8,11},{9,8},{10,9... | collective-permute-start | bytes 1966088 | tf_op jit(solution)/shard_map/ppermute | solution.py:197
  104.9 0.2 add_convert_fusion.1
  105.1 0.1 collective-permute-start.12
  105.2 11.4 %collective-permute-done.8 = bf16[128,2560]{1,0:T(8,128)(2,1)S(1)} collective-permute-done((bf16[128,2560]{1,0:T(8,128)(2,1)S(1)}, bf16[128,2560]{1,0:T(8,128)(2,1)S(1)}, u32[]{:S(2)}, u32[]{:S(2)}) %collective-permute-start.8) | collective-permute-done | bytes 655392 | tf_op jit(solution)/shard_map/ppermute | solution.py:197
  116.6 0.2 add_convert_fusion.3
  116.7 3.8 %collective-permute-start.9 = (bf16[128,2560]{1,0:T(8,128)(2,1)S(1)}, bf16[128,2560]{1,0:T(8,128)(2,1)S(1)}, u32[]{:S(2)}, u32[]{:S(2)}) collective-permute-start(bf16[128,2560]{1,0:T(8,128)(2,1)S(1)} %add_convert_fusion.3), channel_id=1, source_target_pairs={{0,3},{1,0},{2,1},{3,2},{4,7},{5,4},{6,5},{7,6},{8,11},{9,8},{10,9... | collective-permute-start | bytes 1966088 | tf_op jit(solution)/shard_map/ppermute | solution.py:197
  120.5 0.3 fusion.3
  120.9 7.7 %experts.4 = bf16[256,2560]{1,0:T(8,128)(2,1)S(1)} custom-call(bf16[256,2560]{1,0:T(8,128)(2,1)S(1)} %bitcast.29, bf16[2048,1408]{1,0:T(8,128)(2,1)S(1)} %bitcast.36, bf16[2048,1408]{1,0:T(8,128)(2,1)S(1)} %bitcast.40, bf16[1408,2048]{1,0:T(8,128)(2,1)S(1)} %bitcast.44), custom_call_target="tpu_custom_call" | custom-call | flops 5536481280 | bytes 19922944 | tf_op jit(solution)/shard_map/experts/pallas_call | solution.py:167
  128.6 2.5 %collective-permute-done.9 = bf16[128,2560]{1,0:T(8,128)(2,1)S(1)} collective-permute-done((bf16[128,2560]{1,0:T(8,128)(2,1)S(1)}, bf16[128,2560]{1,0:T(8,128)(2,1)S(1)}, u32[]{:S(2)}, u32[]{:S(2)}) %collective-permute-start.9) | collective-permute-done | bytes 655392 | tf_op jit(solution)/shard_map/ppermute | solution.py:197
  131.1 0.5 add_convert_fusion.2
  131.6 1.2 maximum_bitcast_fusion
  132.7 10.8 %all-to-all-start.1 = ((bf16[32,8,2560]{2,1,0:T(8,128)(2,1)}), bf16[32,8,2560]{2,1,0:T(8,128)(2,1)S(1)}, u32[]{:S(2)}, u32[]{:S(2)}) async-start(bf16[32,8,2560]{2,1,0:T(8,128)(2,1)} %maximum_bitcast_fusion), calls=%async_computation.1 | async-start | bytes 2621440 | tf_op jit(solution)/shard_map/all_to_all | solution.py:207
  143.5 0.2 fusion.2
  143.7 3.5 %multiply_reduce_fusion = (f32[256]{0:T(256)S(1)}, f32[256,2048]{1,0:T(8,128)S(1)}) fusion(bf16[256,1024]{0,1:T(8,128)(2,1)S(1)} %fusion.2, bf16[1024,2048]{1,0:T(8,128)(2,1)} %param.16), kind=kOutput, calls=%fused_computation.1 | convolution fusion | flops 1074790144 | bytes 6816768 | tf_op jit(solution)/shard_map/dot_general | solution.py:279
  147.3 1.2 multiply_convert_fusion
  148.6 15.5 %all-to-all-done.1 = bf16[32,8,2560]{2,1,0:T(8,128)(2,1)S(1)} async-done(((bf16[32,8,2560]{2,1,0:T(8,128)(2,1)}), bf16[32,8,2560]{2,1,0:T(8,128)(2,1)S(1)}, u32[]{:S(2)}, u32[]{:S(2)}) %all-to-all-start.1) | async-done | bytes 1310752 | tf_op jit(solution)/shard_map/all_to_all | solution.py:207
  164.1 1.9 %combine.1 = bf16[128,2048]{1,0:T(8,128)(2,1)} custom-call(s32[2,128]{1,0:T(2,128)S(1)} %bitcast.48, f32[2,128]{1,0:T(2,128)S(1)} %bitcast.49, f32[1,2048]{1,0:T(1,128)S(1)} %bitcast.46, bf16[256,2560]{1,0:T(8,128)(2,1)S(1)} %bitcast.30), custom_call_target="tpu_custom_call" | custom-call | flops 1073741824 | bytes 2097152 | tf_op jit(solution)/shard_map/combine/pallas_call | solution.py:241
  (40 shorter events, 0.2 us)
Async XLA Ops:
  0.6 119.9 %copy-start = (bf16[4,256,256]{2,1,0:T(8,128)(2,1)S(1)}, bf16[4,256,256]{2,1,0:T(8,128)(2,1)}, u32[]{:S(2)}) copy-start(bf16[4,256,256]{2,1,0:T(8,128)(2,1)} %param.14) | copy-start | bytes 1572868
  0.6 1.1 copy-start.3
  1.7 0.7 copy-start.4
  2.4 0.7 copy-start.6
  5.1 8.6 %copy-start.9 = (bf16[256,1024]{1,0:T(8,128)(2,1)S(1)}, bf16[256,1024]{1,0:T(8,128)(2,1)}, u32[]{:S(2)}) copy-start(bf16[256,1024]{1,0:T(8,128)(2,1)} %param.13) | copy-start | bytes 1572868
  5.1 29.4 %all-to-all-start = ((bf16[32,8,2560]{2,1,0:T(8,128)(2,1)}), bf16[32,8,2560]{2,1,0:T(8,128)(2,1)S(1)}, u32[]{:S(2)}, u32[]{:S(2)}) async-start(bf16[32,8,2560]{2,1,0:T(8,128)(2,1)} %bitcast.6), calls=%async_computation | async-start | bytes 2621440 | tf_op jit(solution)/shard_map/all_to_all | solution.py:207
  13.7 5.0 %collective-permute-start = (bf16[16,1024]{1,0:T(8,128)(2,1)S(1)}, bf16[16,1024]{1,0:T(8,128)(2,1)S(1)}, u32[]{:S(2)}, u32[]{:S(2)}) collective-permute-start(bf16[16,1024]{1,0:T(8,128)(2,1)S(1)} %slice.59), channel_id=1, source_target_pairs={{0,1},{1,2},{2,3},{3,4},{4,5},{5,6},{6,7},{7,8},{8,9},{9,10},{10,1... | collective-permute-start | bytes 98312 | tf_op jit(solution)/shard_map/ppermute | solution.py:258
  34.6 16.6 %collective-permute-start.4 = (bf16[128,2560]{1,0:T(8,128)(2,1)S(1)}, bf16[128,2560]{1,0:T(8,128)(2,1)S(1)}, u32[]{:S(2)}, u32[]{:S(2)}) collective-permute-start(bf16[128,2560]{1,0:T(8,128)(2,1)S(1)} %get-tuple-element.17), channel_id=1, source_target_pairs={{0,1},{1,2},{2,3},{3,0},{4,5},{5,6},{6,7},{7,4},{8,9},{9,10},{10,1... | collective-permute-start | bytes 1966088 | tf_op jit(solution)/shard_map/ppermute | solution.py:193
  35.9 15.6 %collective-permute-start.5 = (bf16[128,2560]{1,0:T(8,128)(2,1)S(1)}, bf16[128,2560]{1,0:T(8,128)(2,1)S(1)}, u32[]{:S(2)}, u32[]{:S(2)}) collective-permute-start(bf16[128,2560]{1,0:T(8,128)(2,1)S(1)} %get-tuple-element.16), channel_id=1, source_target_pairs={{0,3},{1,0},{2,1},{3,2},{4,7},{5,4},{6,5},{7,6},{8,11},{9,8},{10,9... | collective-permute-start | bytes 1966088 | tf_op jit(solution)/shard_map/ppermute | solution.py:197
  38.2 31.8 %slice-start = ((s8[5767168]{0:T(1024)(128)(4,1)}), s8[4194304]{0:T(1024)(128)(4,1)S(1)}, s32[]{:S(2)}) async-start(s8[5767168]{0:T(1024)(128)(4,1)} %bitcast.31), calls=%async_computation.2 | async-start | bytes 8388608
  38.4 31.6 %slice-start.1 = ((s8[5767168]{0:T(1024)(128)(4,1)}), s8[1572864]{0:T(1024)(128)(4,1)S(1)}, s32[]{:S(2)}) async-start(s8[5767168]{0:T(1024)(128)(4,1)} %bitcast.31), calls=%async_computation.3 | async-start | bytes 3145728
  51.2 18.8 %collective-permute-start.6 = (bf16[128,2560]{1,0:T(8,128)(2,1)S(1)}, bf16[128,2560]{1,0:T(8,128)(2,1)S(1)}, u32[]{:S(2)}, u32[]{:S(2)}) collective-permute-start(bf16[128,2560]{1,0:T(8,128)(2,1)S(1)} %collective-permute-done.4.refs_0_), channel_id=1, source_target_pairs={{0,1},{1,2},{2,3},{3,0},{4,5},{5,6},{6,7},{7,4},{8,9},{9,10},{10,1... | collective-permute-start | bytes 1966088 | tf_op jit(solution)/shard_map/ppermute | solution.py:193
  51.6 18.4 %collective-permute-start.7 = (bf16[128,2560]{1,0:T(8,128)(2,1)S(1)}, bf16[128,2560]{1,0:T(8,128)(2,1)S(1)}, u32[]{:S(2)}, u32[]{:S(2)}) collective-permute-start(bf16[128,2560]{1,0:T(8,128)(2,1)S(1)} %collective-permute-done.5.refs_1_), channel_id=1, source_target_pairs={{0,3},{1,0},{2,1},{3,2},{4,7},{5,4},{6,5},{7,6},{8,11},{9,8},{10,9... | collective-permute-start | bytes 1966088 | tf_op jit(solution)/shard_map/ppermute | solution.py:197
  54.7 29.0 %collective-permute-start.1 = (bf16[128,2560]{1,0:T(8,128)(2,1)S(1)}, bf16[128,2560]{1,0:T(8,128)(2,1)S(1)}, u32[]{:S(2)}, u32[]{:S(2)}) collective-permute-start(bf16[128,2560]{1,0:T(8,128)(2,1)S(1)} %get-tuple-element.16), channel_id=1, source_target_pairs={{0,1},{1,2},{2,3},{3,0},{4,5},{5,6},{6,7},{7,4},{8,9},{9,10},{10,1... | collective-permute-start | bytes 1966088 | tf_op jit(solution)/shard_map/ppermute | solution.py:193
  54.8 29.0 %collective-permute-start.2 = (bf16[128,2560]{1,0:T(8,128)(2,1)S(1)}, bf16[128,2560]{1,0:T(8,128)(2,1)S(1)}, u32[]{:S(2)}, u32[]{:S(2)}) collective-permute-start(bf16[128,2560]{1,0:T(8,128)(2,1)S(1)} %get-tuple-element.17), channel_id=1, source_target_pairs={{0,3},{1,0},{2,1},{3,2},{4,7},{5,4},{6,5},{7,6},{8,11},{9,8},{10,9... | collective-permute-start | bytes 1966088 | tf_op jit(solution)/shard_map/ppermute | solution.py:197
  70.0 2.6 %copy-start.1 = (bf16[1,2048,1408]{2,1,0:T(8,128)(2,1)S(1)}, bf16[1,2048,1408]{2,1,0:T(8,128)(2,1)}, u32[]{:S(2)}) copy-start(bf16[1,2048,1408]{2,1,0:T(8,128)(2,1)} %param.23) | copy-start | bytes 17301508
  72.6 2.6 %copy-start.2 = (bf16[1,1408,2048]{2,1,0:T(8,128)(2,1)S(1)}, bf16[1,1408,2048]{2,1,0:T(8,128)(2,1)}, u32[]{:S(2)}) copy-start(bf16[1,1408,2048]{2,1,0:T(8,128)(2,1)} %param.24) | copy-start | bytes 17301508
  82.9 22.1 %collective-permute-start.11 = (bf16[128,2560]{1,0:T(8,128)(2,1)S(1)}, bf16[128,2560]{1,0:T(8,128)(2,1)S(1)}, u32[]{:S(2)}, u32[]{:S(2)}) collective-permute-start(bf16[128,2560]{1,0:T(8,128)(2,1)S(1)} %get-tuple-element.13), channel_id=1, source_target_pairs={{0,1},{1,2},{2,3},{3,0},{4,5},{5,6},{6,7},{7,4},{8,9},{9,10},{10,1... | collective-permute-start | bytes 1966088 | tf_op jit(solution)/shard_map/ppermute | solution.py:193
  91.4 37.2 %collective-permute-start.10 = (bf16[128,2560]{1,0:T(8,128)(2,1)S(1)}, bf16[128,2560]{1,0:T(8,128)(2,1)S(1)}, u32[]{:S(2)}, u32[]{:S(2)}) collective-permute-start(bf16[128,2560]{1,0:T(8,128)(2,1)S(1)} %get-tuple-element.11), channel_id=1, source_target_pairs={{0,3},{1,0},{2,1},{3,2},{4,7},{5,4},{6,5},{7,6},{8,11},{9,8},{10,9... | collective-permute-start | bytes 1966088 | tf_op jit(solution)/shard_map/ppermute | solution.py:197
  94.0 34.6 %collective-permute-start.3 = (bf16[128,2560]{1,0:T(8,128)(2,1)S(1)}, bf16[128,2560]{1,0:T(8,128)(2,1)S(1)}, u32[]{:S(2)}, u32[]{:S(2)}) collective-permute-start(bf16[128,2560]{1,0:T(8,128)(2,1)S(1)} %get-tuple-element.8), channel_id=1, source_target_pairs={{0,1},{1,2},{2,3},{3,0},{4,5},{5,6},{6,7},{7,4},{8,9},{9,10},{10,1... | collective-permute-start | bytes 1966088 | tf_op jit(solution)/shard_map/ppermute | solution.py:193
  101.6 14.9 %collective-permute-start.8 = (bf16[128,2560]{1,0:T(8,128)(2,1)S(1)}, bf16[128,2560]{1,0:T(8,128)(2,1)S(1)}, u32[]{:S(2)}, u32[]{:S(2)}) collective-permute-start(bf16[128,2560]{1,0:T(8,128)(2,1)S(1)} %get-tuple-element.10), channel_id=1, source_target_pairs={{0,3},{1,0},{2,1},{3,2},{4,7},{5,4},{6,5},{7,6},{8,11},{9,8},{10,9... | collective-permute-start | bytes 1966088 | tf_op jit(solution)/shard_map/ppermute | solution.py:197
  105.1 23.5 %collective-permute-start.12 = (bf16[128,2560]{1,0:T(8,128)(2,1)S(1)}, bf16[128,2560]{1,0:T(8,128)(2,1)S(1)}, u32[]{:S(2)}, u32[]{:S(2)}) collective-permute-start(bf16[128,2560]{1,0:T(8,128)(2,1)S(1)} %add_convert_fusion.1), channel_id=1, source_target_pairs={{0,1},{1,2},{2,3},{3,0},{4,5},{5,6},{6,7},{7,4},{8,9},{9,10},{10,1... | collective-permute-start | bytes 1966088 | tf_op jit(solution)/shard_map/ppermute | solution.py:193
  116.7 14.4 %collective-permute-start.9 = (bf16[128,2560]{1,0:T(8,128)(2,1)S(1)}, bf16[128,2560]{1,0:T(8,128)(2,1)S(1)}, u32[]{:S(2)}, u32[]{:S(2)}) collective-permute-start(bf16[128,2560]{1,0:T(8,128)(2,1)S(1)} %add_convert_fusion.3), channel_id=1, source_target_pairs={{0,3},{1,0},{2,1},{3,2},{4,7},{5,4},{6,5},{7,6},{8,11},{9,8},{10,9... | collective-permute-start | bytes 1966088 | tf_op jit(solution)/shard_map/ppermute | solution.py:197
  132.7 10.8 %copy-start.11 = (f32[1024]{0:T(1024)S(1)}, f32[1024]{0:T(1024)}, u32[]{:S(2)}) copy-start(f32[1024]{0:T(1024)} %param.15) | copy-start | bytes 12292
  132.7 31.3 %all-to-all-start.1 = ((bf16[32,8,2560]{2,1,0:T(8,128)(2,1)}), bf16[32,8,2560]{2,1,0:T(8,128)(2,1)S(1)}, u32[]{:S(2)}, u32[]{:S(2)}) async-start(bf16[32,8,2560]{2,1,0:T(8,128)(2,1)} %maximum_bitcast_fusion), calls=%async_computation.1 | async-start | bytes 2621440 | tf_op jit(solution)/shard_map/all_to_all | solution.py:207
  143.7 3.6 %copy-start.10 = (f32[2048]{0:T(1024)S(1)}, f32[2048]{0:T(1024)}, u32[]{:S(2)}) copy-start(f32[2048]{0:T(1024)} %param.17) | copy-start | bytes 24580
  147.3 16.8 %copy-start.5 = (f32[2048]{0:T(1024)S(1)}, f32[2048]{0:T(1024)}, u32[]{:S(2)}) copy-start(f32[2048]{0:T(1024)} %param.25) | copy-start | bytes 24580
  147.3 16.7 %copy-start.7 = (s32[128,2]{0,1:T(2,128)S(1)}, s32[128,2]{0,1:T(2,128)}, u32[]{:S(2)}) copy-start(s32[128,2]{0,1:T(2,128)} %param.20) | copy-start | bytes 3076
  147.3 16.7 %copy-start.8 = (f32[128,2]{0,1:T(2,128)S(1)}, f32[128,2]{0,1:T(2,128)}, u32[]{:S(2)}) copy-start(f32[128,2]{0,1:T(2,128)} %param.21) | copy-start | bytes 3076

commit v2 on v1

--- a/solution.py
+++ b/solution.py
@@ -66,11 +66,20 @@
     return found
 
 
-def pack_kernel(chunks, routes_ref, rows_ref, gain_ref, *wire_refs):
+def pack_kernel(chunks, *refs):
+    count = len(chunks)
+    sources, wire_refs, buffers, sems = refs[:3], refs[3 : 3 + count], refs[3 + count : 6 + count], refs[6 + count]
+    arrivals = [pltpu.make_async_copy(a, b, sems.at[k]) for k, (a, b) in enumerate(zip(sources, buffers))]
+    for arrival in arrivals:
+        arrival.start()
+    routes_ref, rows_ref, gain_ref = buffers
     experts = wire_refs[0].shape[0] // 8
     tokens = routes_ref.shape[1]
+    arrivals[0].wait()
+    chosen, rank = ranks(experts, routes_ref)
+    for arrival in arrivals[1:]:
+        arrival.wait()
     normed = normalize(rows_ref[...].astype(f32), gain_ref[...]).astype(bf16)
-    chosen, rank = ranks(experts, routes_ref)
     for (parts, _), wire_ref in zip(chunks, wire_refs):
         for part in parts:
             _, _, lane, width = part
@@ -215,9 +224,15 @@
     wires = pl.pallas_call(
         functools.partial(pack_kernel, chunks),
         out_shape=[jax.ShapeDtypeStruct((experts * 8, width), bf16) for _, width in chunks],
-        in_specs=vmem(3),
+        in_specs=[pl.BlockSpec(memory_space=pltpu.HBM)] * 3,
         out_specs=vmem(len(chunks)),
-        compiler_params=pltpu.CompilerParams(vmem_limit_bytes=8 * 2**20),
+        scratch_shapes=[
+            pltpu.VMEM(routes_t.shape, routes_t.dtype),
+            pltpu.VMEM(ffn_in.shape, ffn_in.dtype),
+            pltpu.VMEM((1, features), f32),
+            pltpu.SemaphoreType.DMA((3,)),
+        ],
+        compiler_params=pltpu.CompilerParams(vmem_limit_bytes=60 * 2**20),
         cost_estimate=pl.CostEstimate(flops=2**30, bytes_accessed=2**21, transcendentals=0),
         name="pack",
     )(routes_t, ffn_in, ffn_gain[None])

time: 167 us -> 166 us (level)
  local copies, waits for them, and re-layouts: 8.1 us -> 5.76 us
  Pallas kernels: 34.3 us -> 36 us
    unnamed x28 -> x22, local copies, waits for them, and re-layouts: 7.79 us -> 5.33 us
  transfers between devices with their start and end apart: 15 -> 15, of which waited for: 7 -> 7; matrix products, arithmetic and copies ran while one was open for 4% -> 4% of each run, Pallas kernels for 18% -> 19%
where the time goes in v2:
time: 166 us; the launch traced here: 165 us
  waiting for transfers between devices  70.4 us (42%)
  starting transfers between devices  43.3 us (26%)
  Pallas kernels  36 us (22%)
  local copies, waits for them, and re-layouts  5.76 us (3%)
  other arithmetic  4.34 us (3%)
  matrix products  3.89 us (2%)
    all_to_all x2, waiting for transfers between devices, exchange(): lax.all_to_all(blocks, 'ep', split_axis=0, concat_axis=0, tiled=True)  31.1 us
    pallas_call x4, Pallas kernels, expert_block(): pl.pallas_call(functools.partial(expert_kernel, parts, len(wires)), out_s...  31 us
    ppermute x6, waiting for transfers between devices, rightward(): return lax.ppermute(value, 'tp', ring(1))  24.3 us
    all_to_all x2, starting transfers between devices, exchange(): lax.all_to_all(blocks, 'ep', split_axis=0, concat_axis=0, tiled=True)  19.5 us
    ppermute x6, starting transfers between devices, leftward(): return lax.ppermute(value, 'tp', ring(-1))  17.6 us
    ppermute x6, waiting for transfers between devices, leftward(): return lax.ppermute(value, 'tp', ring(-1))  13.5 us
    unnamed x22, local copies, waits for them, and re-layouts  5.33 us
    dot_general x1, matrix products, pool_mixer(): projected = jnp.dot(pooled, w_out, preferred_element_type=f32)  3.55 us
  transfers between devices with their start and end apart: 15, of which 7 were waited for; matrix products, arithmetic and copies ran while one was open for 4% of the time, Pallas kernels for 19%

profile of v2, /device:TPU:0, one launch (start us, length us, event | category | flops | bytes accessed | tf_op | source)
XLA Modules:
  0.0 164.7 jit_solution(2784370699622347263)
XLA Ops:
  0.6 0.0 copy-start
  0.6 3.1 %pack.1 = bf16[256,2560]{1,0:T(8,128)(2,1)} custom-call(s32[2,128]{1,0:T(2,128)} %bitcast.46, bf16[128,2048]{1,0:T(8,128)(2,1)} %refs_1_.1, f32[1,2048]{1,0:T(1,128)} %bitcast.51), custom_call_target="tpu_custom_call" | custom-call | flops 1073741824 | bytes 2097152 | tf_op jit(solution)/shard_map/pack/pallas_call | solution.py:224
  3.8 8.6 %all-to-all-start = ((bf16[32,8,2560]{2,1,0:T(8,128)(2,1)}), bf16[32,8,2560]{2,1,0:T(8,128)(2,1)S(1)}, u32[]{:S(2)}, u32[]{:S(2)}) async-start(bf16[32,8,2560]{2,1,0:T(8,128)(2,1)} %bitcast.50), calls=%async_computation | async-start | bytes 2621440 | tf_op jit(solution)/shard_map/all_to_all | solution.py:216
  12.4 3.4 %collective-permute-start = (bf16[16,1024]{1,0:T(8,128)(2,1)S(1)}, bf16[16,1024]{1,0:T(8,128)(2,1)S(1)}, u32[]{:S(2)}, u32[]{:S(2)}) collective-permute-start(bf16[16,1024]{1,0:T(8,128)(2,1)S(1)} %slice.59), channel_id=1, source_target_pairs={{0,1},{1,2},{2,3},{3,4},{4,5},{5,6},{6,7},{7,8},{8,9},{9,10},{10,1... | collective-permute-start | bytes 98312 | tf_op jit(solution)/shard_map/ppermute | solution.py:273
  15.8 1.5 collective-permute-done
  17.4 0.1 maximum_convert_fusion
  17.5 15.6 %all-to-all-done = bf16[32,8,2560]{2,1,0:T(8,128)(2,1)S(1)} async-done(((bf16[32,8,2560]{2,1,0:T(8,128)(2,1)}), bf16[32,8,2560]{2,1,0:T(8,128)(2,1)S(1)}, u32[]{:S(2)}, u32[]{:S(2)}) %all-to-all-start) | async-done | bytes 1310752 | tf_op jit(solution)/shard_map/all_to_all | solution.py:216
  33.1 0.1 slice_bitcast_fusion.1
  33.2 1.3 collective-permute-start.4
  34.6 2.0 %collective-permute-start.5 = (bf16[128,2560]{1,0:T(8,128)(2,1)S(1)}, bf16[128,2560]{1,0:T(8,128)(2,1)S(1)}, u32[]{:S(2)}, u32[]{:S(2)}) collective-permute-start(bf16[128,2560]{1,0:T(8,128)(2,1)S(1)} %get-tuple-element.16), channel_id=1, source_target_pairs={{0,3},{1,0},{2,1},{3,2},{4,7},{5,4},{6,5},{7,6},{8,11},{9,8},{10,9... | collective-permute-start | bytes 1966088 | tf_op jit(solution)/shard_map/ppermute | solution.py:206
  36.5 0.1 slice_add_fusion.2
  36.7 0.2 slice_add_fusion.1
  36.9 0.0 slice-start
  36.9 0.2 slice_add_fusion
  37.1 0.0 slice-start.1
  37.1 12.7 %collective-permute-done.4.refs_0_ = bf16[128,2560]{1,0:T(8,128)(2,1)S(1)} collective-permute-done((bf16[128,2560]{1,0:T(8,128)(2,1)S(1)}, bf16[128,2560]{1,0:T(8,128)(2,1)S(1)}, u32[]{:S(2)}, u32[]{:S(2)}) %collective-permute-start.4) | collective-permute-done | bytes 655392 | tf_op jit(solution)/shard_map/ppermute | solution.py:202
  49.8 0.4 collective-permute-start.6
  50.2 2.9 %collective-permute-start.7 = (bf16[128,2560]{1,0:T(8,128)(2,1)S(1)}, bf16[128,2560]{1,0:T(8,128)(2,1)S(1)}, u32[]{:S(2)}, u32[]{:S(2)}) collective-permute-start(bf16[128,2560]{1,0:T(8,128)(2,1)S(1)} %collective-permute-done.5.refs_1_), channel_id=1, source_target_pairs={{0,3},{1,0},{2,1},{3,2},{4,7},{5,4},{6,5},{7,6},{8,11},{9,8},{10,9... | collective-permute-start | bytes 1966088 | tf_op jit(solution)/shard_map/ppermute | solution.py:206
  53.1 0.3 fusion.21
  53.4 0.1 slice_add_fusion.3
  53.5 0.1 collective-permute-start.1
  53.6 3.2 %collective-permute-start.2 = (bf16[128,2560]{1,0:T(8,128)(2,1)S(1)}, bf16[128,2560]{1,0:T(8,128)(2,1)S(1)}, u32[]{:S(2)}, u32[]{:S(2)}) collective-permute-start(bf16[128,2560]{1,0:T(8,128)(2,1)S(1)} %get-tuple-element.17), channel_id=1, source_target_pairs={{0,3},{1,0},{2,1},{3,2},{4,7},{5,4},{6,5},{7,6},{8,11},{9,8},{10,9... | collective-permute-start | bytes 1966088 | tf_op jit(solution)/shard_map/ppermute | solution.py:206
  56.8 0.3 fusion.1
  57.1 11.5 %collective-permute-done.6.refs_0_ = bf16[128,2560]{1,0:T(8,128)(2,1)S(1)} collective-permute-done((bf16[128,2560]{1,0:T(8,128)(2,1)S(1)}, bf16[128,2560]{1,0:T(8,128)(2,1)S(1)}, u32[]{:S(2)}, u32[]{:S(2)}) %collective-permute-start.6) | collective-permute-done | bytes 655392 | tf_op jit(solution)/shard_map/ppermute | solution.py:202
  68.7 2.6 %copy-done.1 = bf16[1,2048,1408]{2,1,0:T(8,128)(2,1)S(1)} copy-done((bf16[1,2048,1408]{2,1,0:T(8,128)(2,1)S(1)}, bf16[1,2048,1408]{2,1,0:T(8,128)(2,1)}, u32[]{:S(2)}) %copy-start.1) | copy-done | bytes 5767192
  71.3 2.6 %copy-done.2 = bf16[1,1408,2048]{2,1,0:T(8,128)(2,1)S(1)} copy-done((bf16[1,1408,2048]{2,1,0:T(8,128)(2,1)S(1)}, bf16[1,1408,2048]{2,1,0:T(8,128)(2,1)}, u32[]{:S(2)}) %copy-start.2) | copy-done | bytes 5767192
  73.9 7.7 %experts.7 = (bf16[128,2560]{1,0:T(8,128)(2,1)S(1)}, bf16[128,2560]{1,0:T(8,128)(2,1)S(1)}) custom-call(bf16[128,2560]{1,0:T(8,128)(2,1)S(1)} %collective-permute-done.6.refs_0_, bf16[128,2560]{1,0:T(8,128)(2,1)S(1)} %collective-permute-done.7.refs_1_, bf16[2048,1408]{1,0:T(8,128)(2,1)S(1)} %bitcast.33, bf16[2048,1408]{1,0:T(8,128)(2,1)S(1)} %bitcast.37, ...), custom_call_target="tpu_custom_call" | custom-call | flops 5536481280 | bytes 19922944 | tf_op jit(solution)/shard_map/experts/pallas_call | solution.py:176
  81.6 0.9 collective-permute-start.11
  82.6 7.7 %experts.5 = (bf16[128,2560]{1,0:T(8,128)(2,1)S(1)}, bf16[128,2560]{1,0:T(8,128)(2,1)S(1)}) custom-call(bf16[128,2560]{1,0:T(8,128)(2,1)S(1)} %collective-permute-done.1.refs_0_, bf16[128,2560]{1,0:T(8,128)(2,1)S(1)} %collective-permute-done.2.refs_1_, bf16[2048,1408]{1,0:T(8,128)(2,1)S(1)} %bitcast.34, bf16[2048,1408]{1,0:T(8,128)(2,1)S(1)} %bitcast.38, ...), custom_call_target="tpu_custom_call" | custom-call | flops 5536481280 | bytes 19922944 | tf_op jit(solution)/shard_map/experts/pallas_call | solution.py:176
  90.3 2.7 %collective-permute-start.10 = (bf16[128,2560]{1,0:T(8,128)(2,1)S(1)}, bf16[128,2560]{1,0:T(8,128)(2,1)S(1)}, u32[]{:S(2)}, u32[]{:S(2)}) collective-permute-start(bf16[128,2560]{1,0:T(8,128)(2,1)S(1)} %get-tuple-element.11), channel_id=1, source_target_pairs={{0,3},{1,0},{2,1},{3,2},{4,7},{5,4},{6,5},{7,6},{8,11},{9,8},{10,9... | collective-permute-start | bytes 1966088 | tf_op jit(solution)/shard_map/ppermute | solution.py:206
  93.0 7.7 %experts.6 = (bf16[128,2560]{1,0:T(8,128)(2,1)S(1)}, bf16[128,2560]{1,0:T(8,128)(2,1)S(1)}) custom-call(bf16[128,2560]{1,0:T(8,128)(2,1)S(1)} %collective-permute-done.4.refs_0_, bf16[128,2560]{1,0:T(8,128)(2,1)S(1)} %collective-permute-done.5.refs_1_, bf16[2048,1408]{1,0:T(8,128)(2,1)S(1)} %bitcast.35, bf16[2048,1408]{1,0:T(8,128)(2,1)S(1)} %bitcast.39, ...), custom_call_target="tpu_custom_call" | custom-call | flops 5536481280 | bytes 19922944 | tf_op jit(solution)/shard_map/experts/pallas_call | solution.py:176
  100.7 3.3 %collective-permute-start.8 = (bf16[128,2560]{1,0:T(8,128)(2,1)S(1)}, bf16[128,2560]{1,0:T(8,128)(2,1)S(1)}, u32[]{:S(2)}, u32[]{:S(2)}) collective-permute-start(bf16[128,2560]{1,0:T(8,128)(2,1)S(1)} %get-tuple-element.10), channel_id=1, source_target_pairs={{0,3},{1,0},{2,1},{3,2},{4,7},{5,4},{6,5},{7,6},{8,11},{9,8},{10,9... | collective-permute-start | bytes 1966088 | tf_op jit(solution)/shard_map/ppermute | solution.py:206
  104.0 0.2 add_convert_fusion.1
  104.2 0.1 collective-permute-start.12
  104.2 11.4 %collective-permute-done.8 = bf16[128,2560]{1,0:T(8,128)(2,1)S(1)} collective-permute-done((bf16[128,2560]{1,0:T(8,128)(2,1)S(1)}, bf16[128,2560]{1,0:T(8,128)(2,1)S(1)}, u32[]{:S(2)}, u32[]{:S(2)}) %collective-permute-start.8) | collective-permute-done | bytes 655392 | tf_op jit(solution)/shard_map/ppermute | solution.py:206
  115.6 0.2 add_convert_fusion.3
  115.8 3.6 %collective-permute-start.9 = (bf16[128,2560]{1,0:T(8,128)(2,1)S(1)}, bf16[128,2560]{1,0:T(8,128)(2,1)S(1)}, u32[]{:S(2)}, u32[]{:S(2)}) collective-permute-start(bf16[128,2560]{1,0:T(8,128)(2,1)S(1)} %add_convert_fusion.3), channel_id=1, source_target_pairs={{0,3},{1,0},{2,1},{3,2},{4,7},{5,4},{6,5},{7,6},{8,11},{9,8},{10,9... | collective-permute-start | bytes 1966088 | tf_op jit(solution)/shard_map/ppermute | solution.py:206
  119.3 0.3 fusion.3
  119.7 7.8 %experts.4 = bf16[256,2560]{1,0:T(8,128)(2,1)S(1)} custom-call(bf16[256,2560]{1,0:T(8,128)(2,1)S(1)} %bitcast.29, bf16[2048,1408]{1,0:T(8,128)(2,1)S(1)} %bitcast.36, bf16[2048,1408]{1,0:T(8,128)(2,1)S(1)} %bitcast.40, bf16[1408,2048]{1,0:T(8,128)(2,1)S(1)} %bitcast.44), custom_call_target="tpu_custom_call" | custom-call | flops 5536481280 | bytes 19922944 | tf_op jit(solution)/shard_map/experts/pallas_call | solution.py:176
  127.5 2.1 %collective-permute-done.9 = bf16[128,2560]{1,0:T(8,128)(2,1)S(1)} collective-permute-done((bf16[128,2560]{1,0:T(8,128)(2,1)S(1)}, bf16[128,2560]{1,0:T(8,128)(2,1)S(1)}, u32[]{:S(2)}, u32[]{:S(2)}) %collective-permute-start.9) | collective-permute-done | bytes 655392 | tf_op jit(solution)/shard_map/ppermute | solution.py:206
  129.6 0.5 add_convert_fusion.2
  130.1 1.2 maximum_bitcast_fusion
  131.3 11.0 %all-to-all-start.1 = ((bf16[32,8,2560]{2,1,0:T(8,128)(2,1)}), bf16[32,8,2560]{2,1,0:T(8,128)(2,1)S(1)}, u32[]{:S(2)}, u32[]{:S(2)}) async-start(bf16[32,8,2560]{2,1,0:T(8,128)(2,1)} %maximum_bitcast_fusion), calls=%async_computation.1 | async-start | bytes 2621440 | tf_op jit(solution)/shard_map/all_to_all | solution.py:216
  142.3 0.2 fusion.2
  142.5 3.5 %multiply_reduce_fusion = (f32[256]{0:T(256)S(1)}, f32[256,2048]{1,0:T(8,128)S(1)}) fusion(bf16[256,1024]{0,1:T(8,128)(2,1)S(1)} %fusion.2, bf16[1024,2048]{1,0:T(8,128)(2,1)} %param.16), kind=kOutput, calls=%fused_computation.1 | convolution fusion | flops 1074790144 | bytes 6816768 | tf_op jit(solution)/shard_map/dot_general | solution.py:294
  146.1 1.2 multiply_convert_fusion
  147.3 15.5 %all-to-all-done.1 = bf16[32,8,2560]{2,1,0:T(8,128)(2,1)S(1)} async-done(((bf16[32,8,2560]{2,1,0:T(8,128)(2,1)}), bf16[32,8,2560]{2,1,0:T(8,128)(2,1)S(1)}, u32[]{:S(2)}, u32[]{:S(2)}) %all-to-all-start.1) | async-done | bytes 1310752 | tf_op jit(solution)/shard_map/all_to_all | solution.py:216
  162.8 1.9 %combine.1 = bf16[128,2048]{1,0:T(8,128)(2,1)} custom-call(s32[2,128]{1,0:T(2,128)S(1)} %bitcast.47, f32[2,128]{1,0:T(2,128)S(1)} %bitcast.48, f32[1,2048]{1,0:T(1,128)S(1)} %bitcast.45, bf16[256,2560]{1,0:T(8,128)(2,1)S(1)} %bitcast.30), custom_call_target="tpu_custom_call" | custom-call | flops 1073741824 | bytes 2097152 | tf_op jit(solution)/shard_map/combine/pallas_call | solution.py:256
  (34 shorter events, 0.2 us)
Async XLA Ops:
  0.6 118.7 %copy-start = (bf16[4,256,256]{2,1,0:T(8,128)(2,1)S(1)}, bf16[4,256,256]{2,1,0:T(8,128)(2,1)}, u32[]{:S(2)}) copy-start(bf16[4,256,256]{2,1,0:T(8,128)(2,1)} %param.14) | copy-start | bytes 1572868
  3.8 8.6 %copy-start.6 = (bf16[256,1024]{1,0:T(8,128)(2,1)S(1)}, bf16[256,1024]{1,0:T(8,128)(2,1)}, u32[]{:S(2)}) copy-start(bf16[256,1024]{1,0:T(8,128)(2,1)} %param.13) | copy-start | bytes 1572868
  3.8 29.4 %all-to-all-start = ((bf16[32,8,2560]{2,1,0:T(8,128)(2,1)}), bf16[32,8,2560]{2,1,0:T(8,128)(2,1)S(1)}, u32[]{:S(2)}, u32[]{:S(2)}) async-start(bf16[32,8,2560]{2,1,0:T(8,128)(2,1)} %bitcast.50), calls=%async_computation | async-start | bytes 2621440 | tf_op jit(solution)/shard_map/all_to_all | solution.py:216
  12.4 5.0 %collective-permute-start = (bf16[16,1024]{1,0:T(8,128)(2,1)S(1)}, bf16[16,1024]{1,0:T(8,128)(2,1)S(1)}, u32[]{:S(2)}, u32[]{:S(2)}) collective-permute-start(bf16[16,1024]{1,0:T(8,128)(2,1)S(1)} %slice.59), channel_id=1, source_target_pairs={{0,1},{1,2},{2,3},{3,4},{4,5},{5,6},{6,7},{7,8},{8,9},{9,10},{10,1... | collective-permute-start | bytes 98312 | tf_op jit(solution)/shard_map/ppermute | solution.py:273
  33.2 16.6 %collective-permute-start.4 = (bf16[128,2560]{1,0:T(8,128)(2,1)S(1)}, bf16[128,2560]{1,0:T(8,128)(2,1)S(1)}, u32[]{:S(2)}, u32[]{:S(2)}) collective-permute-start(bf16[128,2560]{1,0:T(8,128)(2,1)S(1)} %get-tuple-element.17), channel_id=1, source_target_pairs={{0,1},{1,2},{2,3},{3,0},{4,5},{5,6},{6,7},{7,4},{8,9},{9,10},{10,1... | collective-permute-start | bytes 1966088 | tf_op jit(solution)/shard_map/ppermute | solution.py:202
  34.6 15.6 %collective-permute-start.5 = (bf16[128,2560]{1,0:T(8,128)(2,1)S(1)}, bf16[128,2560]{1,0:T(8,128)(2,1)S(1)}, u32[]{:S(2)}, u32[]{:S(2)}) collective-permute-start(bf16[128,2560]{1,0:T(8,128)(2,1)S(1)} %get-tuple-element.16), channel_id=1, source_target_pairs={{0,3},{1,0},{2,1},{3,2},{4,7},{5,4},{6,5},{7,6},{8,11},{9,8},{10,9... | collective-permute-start | bytes 1966088 | tf_op jit(solution)/shard_map/ppermute | solution.py:206
  36.9 31.8 %slice-start = ((s8[5767168]{0:T(1024)(128)(4,1)}), s8[4194304]{0:T(1024)(128)(4,1)S(1)}, s32[]{:S(2)}) async-start(s8[5767168]{0:T(1024)(128)(4,1)} %bitcast.31), calls=%async_computation.2 | async-start | bytes 8388608
  37.1 31.6 %slice-start.1 = ((s8[5767168]{0:T(1024)(128)(4,1)}), s8[1572864]{0:T(1024)(128)(4,1)S(1)}, s32[]{:S(2)}) async-start(s8[5767168]{0:T(1024)(128)(4,1)} %bitcast.31), calls=%async_computation.3 | async-start | bytes 3145728
  49.8 18.8 %collective-permute-start.6 = (bf16[128,2560]{1,0:T(8,128)(2,1)S(1)}, bf16[128,2560]{1,0:T(8,128)(2,1)S(1)}, u32[]{:S(2)}, u32[]{:S(2)}) collective-permute-start(bf16[128,2560]{1,0:T(8,128)(2,1)S(1)} %collective-permute-done.4.refs_0_), channel_id=1, source_target_pairs={{0,1},{1,2},{2,3},{3,0},{4,5},{5,6},{6,7},{7,4},{8,9},{9,10},{10,1... | collective-permute-start | bytes 1966088 | tf_op jit(solution)/shard_map/ppermute | solution.py:202
  50.2 18.4 %collective-permute-start.7 = (bf16[128,2560]{1,0:T(8,128)(2,1)S(1)}, bf16[128,2560]{1,0:T(8,128)(2,1)S(1)}, u32[]{:S(2)}, u32[]{:S(2)}) collective-permute-start(bf16[128,2560]{1,0:T(8,128)(2,1)S(1)} %collective-permute-done.5.refs_1_), channel_id=1, source_target_pairs={{0,3},{1,0},{2,1},{3,2},{4,7},{5,4},{6,5},{7,6},{8,11},{9,8},{10,9... | collective-permute-start | bytes 1966088 | tf_op jit(solution)/shard_map/ppermute | solution.py:206
  53.5 29.0 %collective-permute-start.1 = (bf16[128,2560]{1,0:T(8,128)(2,1)S(1)}, bf16[128,2560]{1,0:T(8,128)(2,1)S(1)}, u32[]{:S(2)}, u32[]{:S(2)}) collective-permute-start(bf16[128,2560]{1,0:T(8,128)(2,1)S(1)} %get-tuple-element.16), channel_id=1, source_target_pairs={{0,1},{1,2},{2,3},{3,0},{4,5},{5,6},{6,7},{7,4},{8,9},{9,10},{10,1... | collective-permute-start | bytes 1966088 | tf_op jit(solution)/shard_map/ppermute | solution.py:202
  53.6 29.0 %collective-permute-start.2 = (bf16[128,2560]{1,0:T(8,128)(2,1)S(1)}, bf16[128,2560]{1,0:T(8,128)(2,1)S(1)}, u32[]{:S(2)}, u32[]{:S(2)}) collective-permute-start(bf16[128,2560]{1,0:T(8,128)(2,1)S(1)} %get-tuple-element.17), channel_id=1, source_target_pairs={{0,3},{1,0},{2,1},{3,2},{4,7},{5,4},{6,5},{7,6},{8,11},{9,8},{10,9... | collective-permute-start | bytes 1966088 | tf_op jit(solution)/shard_map/ppermute | solution.py:206
  68.6 2.6 %copy-start.1 = (bf16[1,2048,1408]{2,1,0:T(8,128)(2,1)S(1)}, bf16[1,2048,1408]{2,1,0:T(8,128)(2,1)}, u32[]{:S(2)}) copy-start(bf16[1,2048,1408]{2,1,0:T(8,128)(2,1)} %param.23) | copy-start | bytes 17301508
  71.3 2.6 %copy-start.2 = (bf16[1,1408,2048]{2,1,0:T(8,128)(2,1)S(1)}, bf16[1,1408,2048]{2,1,0:T(8,128)(2,1)}, u32[]{:S(2)}) copy-start(bf16[1,1408,2048]{2,1,0:T(8,128)(2,1)} %param.24) | copy-start | bytes 17301508
  81.6 22.4 %collective-permute-start.11 = (bf16[128,2560]{1,0:T(8,128)(2,1)S(1)}, bf16[128,2560]{1,0:T(8,128)(2,1)S(1)}, u32[]{:S(2)}, u32[]{:S(2)}) collective-permute-start(bf16[128,2560]{1,0:T(8,128)(2,1)S(1)} %get-tuple-element.13), channel_id=1, source_target_pairs={{0,1},{1,2},{2,3},{3,0},{4,5},{5,6},{6,7},{7,4},{8,9},{9,10},{10,1... | collective-permute-start | bytes 1966088 | tf_op jit(solution)/shard_map/ppermute | solution.py:202
  90.3 37.2 %collective-permute-start.10 = (bf16[128,2560]{1,0:T(8,128)(2,1)S(1)}, bf16[128,2560]{1,0:T(8,128)(2,1)S(1)}, u32[]{:S(2)}, u32[]{:S(2)}) collective-permute-start(bf16[128,2560]{1,0:T(8,128)(2,1)S(1)} %get-tuple-element.11), channel_id=1, source_target_pairs={{0,3},{1,0},{2,1},{3,2},{4,7},{5,4},{6,5},{7,6},{8,11},{9,8},{10,9... | collective-permute-start | bytes 1966088 | tf_op jit(solution)/shard_map/ppermute | solution.py:206
  93.0 34.5 %collective-permute-start.3 = (bf16[128,2560]{1,0:T(8,128)(2,1)S(1)}, bf16[128,2560]{1,0:T(8,128)(2,1)S(1)}, u32[]{:S(2)}, u32[]{:S(2)}) collective-permute-start(bf16[128,2560]{1,0:T(8,128)(2,1)S(1)} %get-tuple-element.8), channel_id=1, source_target_pairs={{0,1},{1,2},{2,3},{3,0},{4,5},{5,6},{6,7},{7,4},{8,9},{9,10},{10,1... | collective-permute-start | bytes 1966088 | tf_op jit(solution)/shard_map/ppermute | solution.py:202
  100.7 14.9 %collective-permute-start.8 = (bf16[128,2560]{1,0:T(8,128)(2,1)S(1)}, bf16[128,2560]{1,0:T(8,128)(2,1)S(1)}, u32[]{:S(2)}, u32[]{:S(2)}) collective-permute-start(bf16[128,2560]{1,0:T(8,128)(2,1)S(1)} %get-tuple-element.10), channel_id=1, source_target_pairs={{0,3},{1,0},{2,1},{3,2},{4,7},{5,4},{6,5},{7,6},{8,11},{9,8},{10,9... | collective-permute-start | bytes 1966088 | tf_op jit(solution)/shard_map/ppermute | solution.py:206
  104.2 23.4 %collective-permute-start.12 = (bf16[128,2560]{1,0:T(8,128)(2,1)S(1)}, bf16[128,2560]{1,0:T(8,128)(2,1)S(1)}, u32[]{:S(2)}, u32[]{:S(2)}) collective-permute-start(bf16[128,2560]{1,0:T(8,128)(2,1)S(1)} %add_convert_fusion.1), channel_id=1, source_target_pairs={{0,1},{1,2},{2,3},{3,0},{4,5},{5,6},{6,7},{7,4},{8,9},{9,10},{10,1... | collective-permute-start | bytes 1966088 | tf_op jit(solution)/shard_map/ppermute | solution.py:202
  115.8 13.9 %collective-permute-start.9 = (bf16[128,2560]{1,0:T(8,128)(2,1)S(1)}, bf16[128,2560]{1,0:T(8,128)(2,1)S(1)}, u32[]{:S(2)}, u32[]{:S(2)}) collective-permute-start(bf16[128,2560]{1,0:T(8,128)(2,1)S(1)} %add_convert_fusion.3), channel_id=1, source_target_pairs={{0,3},{1,0},{2,1},{3,2},{4,7},{5,4},{6,5},{7,6},{8,11},{9,8},{10,9... | collective-permute-start | bytes 1966088 | tf_op jit(solution)/shard_map/ppermute | solution.py:206
  131.3 11.0 %copy-start.8 = (f32[1024]{0:T(1024)S(1)}, f32[1024]{0:T(1024)}, u32[]{:S(2)}) copy-start(f32[1024]{0:T(1024)} %param.15) | copy-start | bytes 12292
  131.3 31.5 %all-to-all-start.1 = ((bf16[32,8,2560]{2,1,0:T(8,128)(2,1)}), bf16[32,8,2560]{2,1,0:T(8,128)(2,1)S(1)}, u32[]{:S(2)}, u32[]{:S(2)}) async-start(bf16[32,8,2560]{2,1,0:T(8,128)(2,1)} %maximum_bitcast_fusion), calls=%async_computation.1 | async-start | bytes 2621440 | tf_op jit(solution)/shard_map/all_to_all | solution.py:216
  142.5 3.6 %copy-start.7 = (f32[2048]{0:T(1024)S(1)}, f32[2048]{0:T(1024)}, u32[]{:S(2)}) copy-start(f32[2048]{0:T(1024)} %param.17) | copy-start | bytes 24580
  146.0 16.8 %copy-start.3 = (f32[2048]{0:T(1024)S(1)}, f32[2048]{0:T(1024)}, u32[]{:S(2)}) copy-start(f32[2048]{0:T(1024)} %param.25) | copy-start | bytes 24580
  146.1 16.7 %copy-start.4 = (s32[128,2]{0,1:T(2,128)S(1)}, s32[128,2]{0,1:T(2,128)}, u32[]{:S(2)}) copy-start(s32[128,2]{0,1:T(2,128)} %param.20) | copy-start | bytes 3076
  146.1 16.7 %copy-start.5 = (f32[128,2]{0,1:T(2,128)S(1)}, f32[128,2]{0,1:T(2,128)}, u32[]{:S(2)}) copy-start(f32[128,2]{0,1:T(2,128)} %param.21) | copy-start | bytes 3076
